TPU v7x, 32 devices: a whole 2x2x4 slice. The times are simulated.
32 devices in a mesh: fs: 8 (over z, x), tp: 4 (over y, core).
Axes of the slice: x: 2, y: 2, z: 4, core: 2. Of those that a mesh axis runs over, the one named last changes fastest.
Arguments:
- mixer_input: bfloat16 [8192, 4096], P('fs'), may hold values from -6 to 6
- cell_output: bfloat16 [8192, 2048], P('fs'), may hold values from -6 to 6
- query_grad: bfloat16 [8192, 2048], P('fs', 'tp'), may hold values from -4 to 4
- value_grad: bfloat16 [8192, 2048], P('fs', 'tp'), may hold values from -4 to 4
- output_grad: bfloat16 [8192, 4096], P('fs', 'tp'), may hold values from -4 to 4
- query_weight: float32 [4096, 2048], P('fs', 'tp'), may hold values from -6 to 6
- value_weight: float32 [4096, 2048], P('fs', 'tp'), may hold values from -6 to 6
- output_weight: float32 [2048, 4096], P('fs', 'tp'), may hold values from -6 to 6
- query_basis: bfloat16 [4096, 128], P('fs'), may hold values from -0.09375 to 0.09375
- value_basis: bfloat16 [4096, 128], P('fs'), may hold values from -0.09375 to 0.09375
- output_basis: bfloat16 [2048, 128], P('fs'), may hold values from -0.125 to 0.125
- query_mean: float32 [128, 2048], P(None, 'tp'), may hold values from -6 to 6
- value_mean: float32 [128, 2048], P(None, 'tp'), may hold values from -6 to 6
- output_mean: float32 [128, 4096], P(None, 'tp'), may hold values from -6 to 6
- query_square: float32 [128, 2048], P(None, 'tp'), may hold values from 0.25 to 4
- value_square: float32 [128, 2048], P(None, 'tp'), may hold values from 0.25 to 4
- output_square: float32 [128, 4096], P(None, 'tp'), may hold values from 0.25 to 4
Outputs:
- query_step: float32 [4096, 2048], P('fs', 'tp')
- value_step: float32 [4096, 2048], P('fs', 'tp')
- output_step: float32 [2048, 4096], P('fs', 'tp')
- query_copy: bfloat16 [4096, 2048], P(None, 'tp')
- value_copy: bfloat16 [4096, 2048], P(None, 'tp')
- output_copy: bfloat16 [2048, 4096], P(None, 'tp')
- query_first: float32 [128, 2048], P(None, 'tp')
- value_first: float32 [128, 2048], P(None, 'tp')
- output_first: float32 [128, 4096], P(None, 'tp')
- query_second: float32 [128, 2048], P(None, 'tp')
- value_second: float32 [128, 2048], P(None, 'tp')
- output_second: float32 [128, 4096], P(None, 'tp')
All inputs are finite; a program needn't handle non-finite values.
Results may differ from a plain program's by a relative error of at most 0.013.
Values may be sent and summed in bfloat16 or wider, within the bound.
A program may use at most 128 MiB of HBM per device.

v0:
```python
import functools

import jax
import jax.numpy as jnp
from jax import lax
from jax.experimental import pallas as pl
from jax.experimental.pallas import tpu as pltpu
from jax.sharding import PartitionSpec as P

MODEL = 4096
CELL = 2048


beta_first = 0.8
beta_second = 0.9
floor_mean = 0.005
learn_rate = 0.05

MESH = pl.DeviceIdType.MESH


def matmul(left, right):
    return jnp.dot(left, right, preferred_element_type=jnp.float32)


def split(value):
    high = lax.reduce_precision(value, 8, 7)
    return high.astype(jnp.bfloat16), (value - high).astype(jnp.bfloat16)


def moments(projected, mean_old, square_old):
    moment_one = beta_first * mean_old + (1.0 - beta_first) * projected
    moment_two = beta_second * square_old + (1.0 - beta_second) * projected * projected
    return (moment_one, moment_two, moment_one / jnp.sqrt(moment_two))


def twice(basis):
    return jnp.concatenate([basis, basis], axis=1)


class Gather:
    def __init__(self, number, own, whole, block, half, me, count, by_line, send_sem, recv_sem):
        self.number, self.whole, self.block, self.half = number, whole, block, half
        self.me, self.count, self.by_line = me, count, by_line
        self.send_sem, self.recv_sem = send_sem, recv_sem
        self.rows = block // 2 if half is not None else block
        self.sent = []
        self.relayed = count == 8
        self.place, self.side = me // 2, lax.rem(me, 2)
        self.own = self.slot(me) if own is None else own

    def index(self, step, other=False):
        place = lax.rem(self.place + step + 4, 4)
        return place * 2 + (1 - self.side if other else self.side)

    def slot(self, origin):
        start = pl.multiple_of(origin * self.block, self.block)
        if self.half:
            start = pl.multiple_of(start + self.rows, self.rows)
        return self.whole.at[pl.ds(start, self.rows), :]

    def send(self, role, origin, target, inside=None, source=None):
        copy = pltpu.make_async_remote_copy(
            src_ref=self.slot(origin) if source is None else source,
            dst_ref=self.slot(origin),
            send_sem=self.send_sem.at[self.number, len(self.sent)],
            recv_sem=self.recv_sem.at[self.number, role],
            device_id={"fs": target},
            device_id_type=MESH,
        )
        self.sent.append((copy, inside))
        if inside is None:
            copy.start()
        else:
            pl.when(inside)(copy.start)

    def arrive(self, role, origin, inside=None):
        copy = pltpu.make_async_remote_copy(
            src_ref=self.slot(origin),
            dst_ref=self.slot(origin),
            send_sem=self.send_sem.at[self.number, 0],
            recv_sem=self.recv_sem.at[self.number, role],
            device_id={"fs": lax.rem(self.me + 1, self.count)},
            device_id_type=MESH,
        )
        if inside is None:
            copy.wait_recv()
        else:
            pl.when(inside)(copy.wait_recv)

    def start(self):
        if self.relayed:
            self.send(0, self.me, self.index(1), self.place < 3, self.own)
            self.send(3, self.me, self.index(-1), self.place > 0, self.own)
            self.send(6, self.me, self.index(0, True), None, self.own)
        else:
            for k in range(1, self.count):
                self.send(k - 1, self.me, lax.rem(self.me + k, self.count), None, self.own)

    def relay(self, distance):
        if not self.relayed:
            return
        place = self.place
        across = not (self.by_line and distance == 1)
        cross = self.index(0, True)
        if not across:
            self.arrive(6, cross)
            self.send(7, cross, self.index(1), place < 3)
            self.send(10, cross, self.index(-1), place > 0)
        below, above = self.index(-distance), self.index(distance)
        from_below, from_above = place >= distance, place + distance < 4
        self.arrive(distance - 1, below, from_below)
        if distance < 3:
            self.send(distance, below, self.index(1), (place >= distance) & (place < 3))
        if across:
            self.send(6 + distance, below, cross, from_below)
        self.arrive(2 + distance, above, from_above)
        if distance < 3:
            self.send(3 + distance, above, self.index(-1), from_above & (place > 0))
        if across:
            self.send(9 + distance, above, cross, from_above)

    def finish(self):
        if not self.relayed:
            for k in range(1, self.count):
                self.arrive(k - 1, lax.rem(self.me + self.count - k, self.count))
            return
        if not self.by_line:
            self.arrive(6, self.index(0, True))
        for distance in range(1, 4):
            self.arrive(6 + distance, self.index(-distance, True), self.place >= distance)
            self.arrive(9 + distance, self.index(distance, True), self.place + distance < 4)

    def drain(self):
        for copy, inside in self.sent:
            if inside is None:
                copy.wait_send()
            else:
                pl.when(inside)(copy.wait_send)


def kernel(
    fs,
    tp,
    mixer_hbm,
    cell_hbm,
    qg_hbm,
    vg_hbm,
    og_hbm,
    pair_hbm,
    ob_hbm,
    qw_hbm,
    vw_hbm,
    ow_hbm,
    qm,
    vm,
    om,
    qs,
    vs,
    os,
    qw_all,
    vw_all,
    ow_all,
    pair_all,
    ob_all,
    proj,
    squares,
    mixer,
    cell,
    qg,
    vg,
    og,
    qw,
    vw,
    ow,
    part,
    parts,
    square_own,
    square_in,
    send_sem,
    recv_sem,
    sum_send,
    sum_recv,
    tp_send,
    tp_recv,
    local_sem,
):
    me, column = lax.axis_index("fs"), lax.axis_index("tp")
    rank, width = qm.shape
    gathers = [
        Gather(0, None, pair_all, pair_hbm.shape[0], None, me, fs, False, send_sem, recv_sem),
        Gather(1, None, ob_all, ob_hbm.shape[0], None, me, fs, True, send_sem, recv_sem),
    ]
    kept = ((qw, qw_all), (vw, vw_all), (ow, ow_all))
    for own, whole in kept:
        block = own.shape[0]
        for half in range(2):
            piece = own.at[pl.ds(half * (block // 2), block // 2), :]
            gathers.append(
                Gather(
                    len(gathers), piece, whole, block, half, me, fs, half == 0, send_sem, recv_sem
                )
            )
    loads = [
        pltpu.make_async_copy(source, target, local_sem.at[i])
        for i, (source, target) in enumerate(
            (
                (pair_hbm, gathers[0].own),
                (ob_hbm, gathers[1].own),
                (qw_hbm, qw),
                (vw_hbm, vw),
                (ow_hbm, ow),
                (cell_hbm, cell),
                (og_hbm, og),
                (mixer_hbm, mixer),
                (qg_hbm, qg),
                (vg_hbm, vg),
            )
        )
    ]
    for load in loads:
        load.start()

    barrier = pltpu.get_barrier_semaphore()
    for k in range(1, fs):
        pl.semaphore_signal(
            barrier, inc=1, device_id={"fs": lax.rem(me + k, fs)}, device_id_type=MESH
        )
    for k in range(1, tp):
        pl.semaphore_signal(
            barrier, inc=1, device_id={"tp": lax.rem(column + k, tp)}, device_id_type=MESH
        )
    pl.semaphore_wait(barrier, fs + tp - 2)

    loads[0].wait()
    gathers[0].start()
    loads[1].wait()
    gathers[1].start()
    loads[2].wait()
    gathers[2].start()
    for distance in range(1, 4):
        gathers[0].relay(distance)
        gathers[1].relay(distance)
    gathers[3].start()
    loads[3].wait()
    gathers[4].start()
    gathers[5].start()
    loads[4].wait()
    gathers[6].start()
    gathers[7].start()
    keeps = []
    for i, (own, whole) in enumerate(kept):
        rows = own.shape[0]
        place = whole.at[pl.ds(pl.multiple_of(me * rows, rows), rows), :]
        keeps.append(pltpu.make_async_copy(own, place, local_sem.at[10 + i]))
    for keep in keeps:
        keep.start()
    gathers[2].relay(1)
    for load in loads[5:]:
        load.wait()
    part[...] = jnp.zeros_like(part)
    gathers[0].finish()
    gathers[1].finish()

    tile = 256

    def project(rows, grad):
        turned = jnp.transpose(rows)
        high = turned.astype(jnp.bfloat16)
        low = (turned - high.astype(jnp.float32)).astype(jnp.bfloat16)
        both = matmul(jnp.concatenate([high, low], axis=0), grad)
        return both[:rank] + both[rank:]

    def step(t, carry):
        at = pl.ds(pl.multiple_of(t * tile, tile), tile)
        rows = matmul(mixer[at, :], pair_all[...])
        part[:, :width] += project(rows[:, :rank], qg[at, :])
        part[:, width : 2 * width] += project(rows[:, rank:], vg[at, :])
        part[:, 2 * width :] += project(matmul(cell[at, :], ob_all[...]), og[at, :])
        return carry

    lax.fori_loop(0, mixer.shape[0] // tile, step, 0)

    share = rank // fs

    def strip(index):
        return pl.ds(pl.multiple_of(index * share, share), share)

    sums = []
    for k in range(1, fs):
        target = lax.rem(me + k, fs)
        copy = pltpu.make_async_remote_copy(
            src_ref=part.at[strip(target), :],
            dst_ref=parts.at[k - 1],
            send_sem=sum_send.at[k - 1],
            recv_sem=sum_recv.at[k - 1],
            device_id={"fs": target},
            device_id_type=MESH,
        )
        copy.start()
        sums.append(copy)
    gathers[3].relay(1)
    gathers[2].relay(2)
    gathers[4].relay(1)
    gathers[3].relay(2)
    gathers[2].relay(3)

    def gram(whole, block):
        def add(i, total):
            piece = whole[pl.ds(pl.multiple_of(i * block, block), block), :]
            turned = jnp.transpose(piece.astype(jnp.float32)).astype(jnp.bfloat16)
            return total + matmul(turned, piece)

        size = whole.shape[1]
        return lax.fori_loop(
            0, whole.shape[0] // block, add, jnp.zeros((size, size), jnp.float32)
        )

    for copy in sums:
        copy.wait_recv()
    total = part[strip(me), :]
    for k in range(1, fs):
        total = total + parts[k - 1]
    proj[strip(me), :] = total
    gram_pair = gram(pair_all, 256)
    gram_output = gram(ob_all, 256)
    strips = Gather(8, None, proj, share, None, me, fs, False, send_sem, recv_sem)
    strips.start()
    gathers[5].relay(1)
    strips.relay(1)
    gathers[4].relay(2)
    gathers[3].relay(3)
    strips.relay(2)
    gathers[6].relay(1)
    gathers[5].relay(2)
    strips.relay(3)
    gathers[4].relay(3)
    gathers[7].relay(1)
    strips.finish()

    def norm(basis_gram, projected, mean, square):
        direction = moments(projected, mean[...], square[...])[2]
        turned = jnp.dot(
            basis_gram,
            direction,
            precision=lax.Precision.HIGHEST,
            preferred_element_type=jnp.float32,
        )
        lanes = jnp.sum(direction * turned, axis=0, keepdims=True)
        return jnp.sum(lanes, axis=1, keepdims=True)

    partial = (
        norm(gram_pair[:rank, :rank], proj[:, :width], qm, qs)
        + norm(gram_pair[rank:, rank:], proj[:, width : 2 * width], vm, vs)
        + norm(gram_output, proj[:, 2 * width :], om, os)
    )
    square_own[...] = jnp.broadcast_to(partial, square_own.shape)
    shares = []
    for k in range(1, tp):
        copy = pltpu.make_async_remote_copy(
            src_ref=square_own,
            dst_ref=square_in.at[k - 1],
            send_sem=tp_send.at[k - 1],
            recv_sem=tp_recv.at[k - 1],
            device_id={"tp": lax.rem(column + k, tp)},
            device_id_type=MESH,
        )
        copy.start()
        shares.append(copy)
    gathers[6].relay(2)
    gathers[5].relay(3)
    gathers[7].relay(2)
    gathers[6].relay(3)
    gathers[7].relay(3)
    for copy in shares:
        copy.wait_recv()
    whole_squares = square_own[...]
    for k in range(1, tp):
        whole_squares = whole_squares + square_in[k - 1]
    squares[...] = whole_squares
    for gather in gathers[2:]:
        gather.finish()
    for copy in sums + shares:
        copy.wait_send()
    for gather in gathers + [strips]:
        gather.drain()
    for keep in keeps:
        keep.wait()


def exchange(fs, tp, mixer, cell, grads, pair, output_basis, weights, means, olds):
    share = pair.shape[1] // 2 // fs
    total = sum(grad.shape[1] for grad in grads)
    rank = means[0].shape[0]
    bf16, f32 = jnp.bfloat16, jnp.float32
    places = max(fs - 1, 16)
    hbm, vmem = pl.BlockSpec(memory_space=pl.ANY), pl.BlockSpec(memory_space=pltpu.VMEM)
    dma = pltpu.SemaphoreType.DMA

    def whole(array):
        return jax.ShapeDtypeStruct((array.shape[0] * fs, array.shape[1]), bf16)

    return pl.pallas_call(
        functools.partial(kernel, fs, tp),
        out_shape=(
            *(whole(weight) for weight in weights),
            whole(pair),
            whole(output_basis),
            jax.ShapeDtypeStruct((rank, total), f32),
            jax.ShapeDtypeStruct((8, 128), f32),
        ),
        in_specs=[hbm] * 10 + [vmem] * 6,
        out_specs=(hbm,) * 3 + (vmem,) * 4,
        scratch_shapes=[
            *(pltpu.VMEM(array.shape, bf16) for array in (mixer, cell, *grads, *weights)),
            pltpu.VMEM((rank, total), f32),
            pltpu.VMEM((fs - 1, share, total), f32),
            pltpu.VMEM((8, 128), f32),
            pltpu.VMEM((tp - 1, 8, 128), f32),
            dma((9, places)),
            dma((9, places)),
            dma((fs - 1,)),
            dma((fs - 1,)),
            dma((tp - 1,)),
            dma((tp - 1,)),
            dma((13,)),
        ],
        compiler_params=pltpu.CompilerParams(
            collective_id=0, has_side_effects=True, vmem_limit_bytes=50 * 1024 * 1024
        ),
    )(mixer, cell, *grads, pair, output_basis, *weights, *means, *olds)


def body(fs, tp):
    def local(
        mixer_input,
        cell_output,
        query_grad,
        value_grad,
        output_grad,
        query_weight,
        value_weight,
        output_weight,
        query_basis,
        value_basis,
        output_basis,
        query_mean,
        value_mean,
        output_mean,
        query_square,
        value_square,
        output_square,
    ):
        rank = query_basis.shape[1]
        means = (query_mean, value_mean, output_mean)
        olds = (query_square, value_square, output_square)
        *weights, whole_pair, whole_output, projected, squares = exchange(
            fs,
            tp,
            mixer_input,
            cell_output,
            (query_grad, value_grad, output_grad),
            jnp.concatenate([query_basis, value_basis], axis=1),
            output_basis,
            [w.astype(jnp.bfloat16) for w in (query_weight, value_weight, output_weight)],
            means,
            olds,
        )
        width = query_grad.shape[1]
        proj = (
            projected[:, :width],
            projected[:, width : 2 * width],
            projected[:, 2 * width :],
        )
        firsts, seconds, dirs = zip(*(moments(*each) for each in zip(proj, means, olds)))
        bases = (whole_pair[:, :rank], whole_pair[:, rank:], whole_output)
        factor = 1.0 / jnp.sqrt(squares[0, 0] / (3.0 * MODEL * CELL) + floor_mean)
        pairs = [jnp.concatenate(split(d), axis=0) for d in dirs]
        steps = [
            -factor * matmul(twice(b), d)
            for b, d in zip((query_basis, value_basis, output_basis), pairs)
        ]
        copies = [
            (w.astype(jnp.float32) + (-learn_rate * factor) * matmul(twice(b), d)).astype(
                jnp.bfloat16
            )
            for w, b, d in zip(weights, bases, pairs)
        ]
        return (*steps, *copies, *firsts, *seconds)

    return local


def solution(mesh):
    rows, split_both, columns = P("fs", None), P("fs", "tp"), P(None, "tp")
    in_specs = (rows,) * 2 + (split_both,) * 6 + (rows,) * 3 + (columns,) * 6
    out_specs = (split_both,) * 3 + (columns,) * 9
    return jax.shard_map(
        body(mesh.shape["fs"], mesh.shape["tp"]),
        mesh=mesh,
        in_specs=in_specs,
        out_specs=out_specs,
        check_vma=False,
    )
```

profile of v0, /device:TPU:0, one launch (start us, length us, event | category | flops | bytes accessed | tf_op | source)
XLA Modules:
  0.0 215.6 jit_solution(13070214668649573630)
XLA Ops:
  0.6 0.0 copy-start.16
  0.7 0.0 copy-start.15
  0.7 0.0 copy-start.5
  0.7 0.0 copy-start.1
  0.7 0.0 copy-start.2
  0.7 0.0 copy-start
  0.7 0.0 copy-start.3
  0.7 0.0 copy-start.4
  0.7 1.4 convert_element_type.45.qw_hbm
  2.2 1.3 convert_element_type.46.vw_hbm
  3.4 1.3 convert_element_type.47.ow_hbm
  4.8 0.0 copy-done.16
  4.8 0.0 copy-done.15
  4.8 0.0 copy-done.5
  4.8 0.0 copy-done.1
  4.8 0.0 copy-done.2
  4.8 0.0 copy-done
  4.8 0.0 copy-done.3
  4.9 0.0 copy-done.4
  4.9 193.2 %shard_map.256 = (bf16[4096,512]{1,0:T(8,128)(2,1)}, bf16[4096,512]{1,0:T(8,128)(2,1)}, bf16[2048,1024]{1,0:T(8,128)(2,1)}, bf16[4096,256]{1,0:T(8,128)(2,1)}, b...) custom-call(bf16[1024,4096]{1,0:T(8,128)(2,1)} %mixer_hbm.1, bf16[1024,2048]{1,0:T(8,128)(2,1)} %cell_hbm.1, ...), custom_call_target="tpu_custom_call" | custom-call | tf_op jit(solution)/shard_map/pallas_call | solution.py:403
  198.1 0.0 copy-start.6
  198.1 0.0 copy-start.19
  198.1 1.4 reduce-precision_convert_fusion.1
  199.5 0.0 copy-start.11
  199.5 0.0 copy-start.12
  199.5 0.0 copy-start.13
  199.6 0.0 copy-start.14
  199.6 0.1 fusion.11
  199.7 0.5 slice.18
  201.2 0.0 copy-done.6
  201.2 0.1 fusion.29
  201.3 0.1 copy-done.19
  201.5 3.3 %add_convert_fusion.1 = bf16[4096,512]{1,0:T(8,128)(2,1)} fusion(bf16[4096,512]{1,0:T(8,128)(2,1)S(1)} %copy-done.19, f32[]{:T(128)} %bitcast.1, bf16[4096,128]{1,0:T(8,128)(2,1)S(1)} %get-tuple-element.35, bf16[128,512]{1,0:T(8,128)(2,1)S(1)} %get-tuple-element.41, bf16[128,512]{1,0:T(8,128)(2,1)S(1)} %get-tuple-element.29), kind=kOutput, calls=%fused_computation.1 | convolution fusion | flops 1086849024 | bytes 9699332 | tf_op jit(solution)/shard_map/dot_general | solution.py:23
  204.7 0.0 copy-done.11
  204.7 0.0 copy-done.12
  204.7 0.0 copy-done.13
  204.8 0.0 copy-start.7
  204.8 0.0 copy-start.10
  204.8 3.3 %add_convert_fusion.2 = bf16[4096,512]{1,0:T(8,128)(2,1)} fusion(bf16[4096,512]{1,0:T(8,128)(2,1)S(1)} %copy-done.18, f32[]{:T(128)} %bitcast.1, bf16[4096,128]{1,0:T(8,128)(2,1)S(1)} %get-tuple-element.36, bf16[128,512]{1,0:T(8,128)(2,1)S(1)} %get-tuple-element.40, bf16[128,512]{1,0:T(8,128)(2,1)S(1)} %get-tuple-element.37), kind=kOutput, calls=%fused_computation.2 | convolution fusion | flops 1086849024 | bytes 9699332 | tf_op jit(solution)/shard_map/dot_general | solution.py:23
  208.1 1.3 convolution_multiply_fusion.1
  209.3 1.3 convolution_multiply_fusion.2
  210.6 0.3 reduce-precision_convert_fusion
  210.9 0.0 copy-start.8
  210.9 0.0 copy-start.9
  210.9 0.1 fusion.9
  211.0 3.3 %add_convert_fusion = bf16[2048,1024]{1,0:T(8,128)(2,1)} fusion(bf16[2048,1024]{1,0:T(8,128)(2,1)S(1)} %copy-done.17, f32[]{:T(128)} %bitcast.1, bf16[2048,128]{1,0:T(8,128)(2,1)S(1)} %get-tuple-element.25, bf16[128,1024]{1,0:T(8,128)(2,1)S(1)} %fusion.9, bf16[128,1024]{1,0:T(8,128)(2,1)S(1)} %get-tuple-element.26), kind=kOutput, calls=%fused_computation | convolution fusion | flops 1085276160 | bytes 9437188 | tf_op jit(solution)/shard_map/dot_general | solution.py:23
  214.3 0.0 copy-done.8
  214.3 1.3 convolution_multiply_fusion
  (9 shorter events, 0.0 us)
Async XLA Ops:
  0.6 4.1 %copy-start.16 = (bf16[512,128]{1,0:T(8,128)(2,1)S(1)}, bf16[512,128]{1,0:T(8,128)(2,1)}, u32[]{:S(2)}) copy-start(bf16[512,128]{1,0:T(8,128)(2,1)} %param.25) | copy-start | bytes 393220
  0.7 4.1 %copy-start.15 = (bf16[512,128]{1,0:T(8,128)(2,1)S(1)}, bf16[512,128]{1,0:T(8,128)(2,1)}, u32[]{:S(2)}) copy-start(bf16[512,128]{1,0:T(8,128)(2,1)} %param.26) | copy-start | bytes 393220
  0.7 4.1 %copy-start.5 = (bf16[256,128]{1,0:T(8,128)(2,1)S(1)}, bf16[256,128]{1,0:T(8,128)(2,1)}, u32[]{:S(2)}) copy-start(bf16[256,128]{1,0:T(8,128)(2,1)} %ob_hbm.1) | copy-start | bytes 196612
  0.7 4.1 %copy-start.1 = (f32[128,512]{1,0:T(8,128)S(1)}, f32[128,512]{1,0:T(8,128)}, u32[]{:S(2)}) copy-start(f32[128,512]{1,0:T(8,128)} %qm.1) | copy-start | bytes 786436
  0.7 4.1 %copy-start.2 = (f32[128,512]{1,0:T(8,128)S(1)}, f32[128,512]{1,0:T(8,128)}, u32[]{:S(2)}) copy-start(f32[128,512]{1,0:T(8,128)} %vm.1) | copy-start | bytes 786436
  0.7 4.1 %copy-start = (f32[128,1024]{1,0:T(8,128)S(1)}, f32[128,1024]{1,0:T(8,128)}, u32[]{:S(2)}) copy-start(f32[128,1024]{1,0:T(8,128)} %om.1) | copy-start | bytes 1572868
  0.7 4.1 %copy-start.3 = (f32[128,512]{1,0:T(8,128)S(1)}, f32[128,512]{1,0:T(8,128)}, u32[]{:S(2)}) copy-start(f32[128,512]{1,0:T(8,128)} %qs.1) | copy-start | bytes 786436
  0.7 4.1 %copy-start.4 = (f32[128,512]{1,0:T(8,128)S(1)}, f32[128,512]{1,0:T(8,128)}, u32[]{:S(2)}) copy-start(f32[128,512]{1,0:T(8,128)} %vs.1) | copy-start | bytes 786436
  198.1 3.1 %copy-start.6 = (bf16[4096,256]{1,0:T(8,128)(2,1)S(1)}, bf16[4096,256]{1,0:T(8,128)(2,1)}, u32[]{:S(2)}) copy-start(bf16[4096,256]{1,0:T(8,128)(2,1)} %get-tuple-element.22) | copy-start | bytes 6291460
  198.1 3.4 %copy-start.19 = (bf16[4096,512]{1,0:T(8,128)(2,1)S(1)}, bf16[4096,512]{1,0:T(8,128)(2,1)}, u32[]{:S(2)}) copy-start(bf16[4096,512]{1,0:T(8,128)(2,1)} %get-tuple-element.23) | copy-start | bytes 12582916
  199.5 5.2 %copy-start.11 = (f32[128,512]{1,0:T(8,128)}, f32[128,512]{1,0:T(8,128)S(1)}, u32[]{:S(2)}) copy-start(f32[128,512]{1,0:T(8,128)S(1)} %get-tuple-element.30) | copy-start | bytes 786436
  199.5 5.2 %copy-start.12 = (f32[128,512]{1,0:T(8,128)}, f32[128,512]{1,0:T(8,128)S(1)}, u32[]{:S(2)}) copy-start(f32[128,512]{1,0:T(8,128)S(1)} %get-tuple-element.31) | copy-start | bytes 786436
  199.5 5.2 %copy-start.13 = (f32[128,512]{1,0:T(8,128)}, f32[128,512]{1,0:T(8,128)S(1)}, u32[]{:S(2)}) copy-start(f32[128,512]{1,0:T(8,128)S(1)} %get-tuple-element.38) | copy-start | bytes 786436
  199.6 5.2 %copy-start.14 = (f32[128,512]{1,0:T(8,128)}, f32[128,512]{1,0:T(8,128)S(1)}, u32[]{:S(2)}) copy-start(f32[128,512]{1,0:T(8,128)S(1)} %get-tuple-element.39) | copy-start | bytes 786436
  201.5 3.3 %copy-start.18 = (bf16[4096,512]{1,0:T(8,128)(2,1)S(1)}, bf16[4096,512]{1,0:T(8,128)(2,1)}, u32[]{:S(2)}) copy-start(bf16[4096,512]{1,0:T(8,128)(2,1)} %get-tuple-element.21) | copy-start | bytes 12582916
  204.8 5.8 %copy-start.7 = (f32[128,1024]{1,0:T(8,128)S(1)}, f32[128,1024]{1,0:T(8,128)}, u32[]{:S(2)}) copy-start(f32[128,1024]{1,0:T(8,128)} %os.1) | copy-start | bytes 1572868
  204.8 5.8 %copy-start.10 = (f32[128,2048]{1,0:T(8,128)S(1)}, f32[128,2048]{1,0:T(8,128)}, u32[]{:S(2)}) copy-start(f32[128,2048]{1,0:T(8,128)} %get-tuple-element.20) | copy-start | bytes 3145732
  208.1 3.0 %copy-start.17 = (bf16[2048,1024]{1,0:T(8,128)(2,1)S(1)}, bf16[2048,1024]{1,0:T(8,128)(2,1)}, u32[]{:S(2)}) copy-start(bf16[2048,1024]{1,0:T(8,128)(2,1)} %get-tuple-element.24) | copy-start | bytes 12582916
  210.9 3.4 %copy-start.8 = (f32[128,1024]{1,0:T(8,128)}, f32[128,1024]{1,0:T(8,128)S(1)}, u32[]{:S(2)}) copy-start(f32[128,1024]{1,0:T(8,128)S(1)} %get-tuple-element.27) | copy-start | bytes 1572868
  210.9 3.4 %copy-start.9 = (f32[128,1024]{1,0:T(8,128)}, f32[128,1024]{1,0:T(8,128)S(1)}, u32[]{:S(2)}) copy-start(f32[128,1024]{1,0:T(8,128)S(1)} %get-tuple-element.28) | copy-start | bytes 1572868
where the time goes:
time: 216 us
  Pallas kernels  193 us (89%)
  matrix products  13.6 us (6%)
  other arithmetic  5.92 us (3%)
    pallas_call x1, Pallas kernels, exchange(): pl.pallas_call(functools.partial(kernel, fs, tp), out_shape=(*(whole(weig...  193 us
    dot_general x6, matrix products, matmul(): return jnp.dot(left, right, preferred_element_type=jnp.float32)  13.6 us

commit v1 on v0

v1 whole, which is shorter than its diff:
```python
import functools

import jax
import jax.numpy as jnp
from jax import lax
from jax.experimental import pallas as pl
from jax.experimental.pallas import tpu as pltpu
from jax.sharding import PartitionSpec as P

beta_first = 0.8
beta_second = 0.9
floor_mean = 0.005
learn_rate = 0.05

MESH = pl.DeviceIdType.MESH
LINE_CHUNKS = 5
CHUNKS = 4


def matmul(left, right):
    return jnp.dot(left, right, preferred_element_type=jnp.float32)


def moments(projected, mean_old, square_old):
    moment_one = beta_first * mean_old + (1.0 - beta_first) * projected
    moment_two = beta_second * square_old + (1.0 - beta_second) * projected * projected
    return (moment_one, moment_two, moment_one / jnp.sqrt(moment_two))


def aligned(start, size):
    return pl.ds(pl.multiple_of(start, size), size)


class Weights:
    def __init__(self, wholes, fs, me, send_sem, recv_sem):
        self.wholes, self.fs, self.me = wholes, fs, me
        self.send_sem, self.recv_sem = send_sem, recv_sem
        self.relayed = fs == 8
        self.place, self.side = me // 2, lax.rem(me, 2)

    def index(self, step, other=False):
        place = lax.rem(self.place + step + 4, 4)
        return place * 2 + (1 - self.side if other else self.side)

    def slot(self, w, i, origin):
        whole = self.wholes[w]
        block = whole.shape[0] // self.fs
        rows = block // CHUNKS
        return whole.at[aligned(origin * block + i * rows, rows), :]

    def copy(self, w, i, origin, site, role, target):
        return pltpu.make_async_remote_copy(
            src_ref=self.slot(w, i, origin),
            dst_ref=self.slot(w, i, origin),
            send_sem=self.send_sem.at[w, i, site],
            recv_sem=self.recv_sem.at[w, i, role],
            device_id={"fs": target},
            device_id_type=MESH,
        )

    def arrive(self, w, i, origin, role, inside):
        copy = self.copy(w, i, origin, 0, role, lax.rem(self.me + 1, self.fs))
        if inside is True:
            copy.wait_recv()
        else:
            pl.when(inside)(copy.wait_recv)

    def sites(self, w, i):
        p = self.place
        line = i * len(self.wholes) + w < LINE_CHUNKS
        out = [
            (0, self.me, 0, self.index(1), p < 3),
            (1, self.me, 3, self.index(-1), p > 0),
            (2, self.me, 6, self.index(0, True), True),
        ]
        cross = self.index(0, True)
        for d in (1, 2):
            out.append((2 + d, self.index(-d), d, self.index(1), (p >= d) & (p < 3)))
            out.append((4 + d, self.index(d), 3 + d, self.index(-1), (p + d < 4) & (p > 0)))
        for d in (1, 2, 3):
            below, above = p >= d, p + d < 4
            if d == 1:
                below = below & jnp.logical_not(line | (p == 1))
                above = above & jnp.logical_not(line | (p == 2))
            out.append((6 + d, self.index(-d), 6 + d, cross, below))
            out.append((9 + d, self.index(d), 9 + d, cross, above))
        out.append((13, cross, 7, self.index(1), (p < 3) & (line | (p == 0))))
        out.append((14, cross, 10, self.index(-1), (p > 0) & (line | (p == 3))))
        return {site[0]: site for site in out}

    def direct(self, w, i):
        return {
            k - 1: (k - 1, self.me, k - 1, lax.rem(self.me + k, self.fs), True)
            for k in range(1, self.fs)
        }

    def send(self, w, i, *wanted):
        table = self.sites(w, i)
        for site in wanted:
            number, origin, role, target, inside = table[site]
            copy = self.copy(w, i, origin, number, role, target)
            if inside is True:
                copy.start()
            else:
                pl.when(inside)(copy.start)

    def each(self, step):
        def chunk(i, carry):
            for w in range(len(self.wholes)):
                step(w, i)
            return carry

        lax.fori_loop(0, CHUNKS, chunk, 0)

    def start(self):
        def step(w, i):
            if self.relayed:
                self.send(w, i, 0, 1, 2)
            else:
                for number, origin, role, target, _ in self.direct(w, i).values():
                    self.copy(w, i, origin, number, role, target).start()

        self.each(step)

    def relay(self, d):
        if not self.relayed:
            return
        p = self.place

        def step(w, i):
            self.arrive(w, i, self.index(-d), d - 1, p >= d)
            self.send(w, i, *((2 + d, 6 + d) if d < 3 else (6 + d,)))
            self.arrive(w, i, self.index(d), 2 + d, p + d < 4)
            self.send(w, i, *((4 + d, 9 + d) if d < 3 else (9 + d,)))

        self.each(step)

    def relay_cross(self):
        if not self.relayed:
            return

        def step(w, i):
            self.arrive(w, i, self.index(0, True), 6, True)
            self.send(w, i, 13, 14)

        self.each(step)

    def finish(self):
        p = self.place

        def step(w, i):
            if not self.relayed:
                for k in range(1, self.fs):
                    self.arrive(w, i, lax.rem(self.me + self.fs - k, self.fs), k - 1, True)
                for number, origin, role, target, _ in self.direct(w, i).values():
                    self.copy(w, i, origin, number, role, target).wait_send()
                return
            for d in (1, 2, 3):
                self.arrive(w, i, self.index(-d, True), 6 + d, p >= d)
                self.arrive(w, i, self.index(d, True), 9 + d, p + d < 4)
            for number, origin, role, target, inside in self.sites(w, i).values():
                copy = self.copy(w, i, origin, number, role, target)
                if inside is True:
                    copy.wait_send()
                else:
                    pl.when(inside)(copy.wait_send)

        self.each(step)


def remote(ref_from, ref_to, send, recv, **device):
    return pltpu.make_async_remote_copy(
        src_ref=ref_from,
        dst_ref=ref_to,
        send_sem=send,
        recv_sem=recv,
        device_id=device,
        device_id_type=MESH,
    )


def kernel(
    fs,
    tp,
    owners,
    mixer_hbm,
    cell_hbm,
    qg_hbm,
    vg_hbm,
    og_hbm,
    qb_hbm,
    vb_hbm,
    ob_hbm,
    qw_hbm,
    vw_hbm,
    ow_hbm,
    qm,
    vm,
    om,
    qs,
    vs,
    os,
    qw_all,
    vw_all,
    ow_all,
    pair_all,
    ob_all,
    proj,
    squares,
    mixer,
    cell,
    qg,
    vg,
    og,
    qw,
    vw,
    ow,
    part,
    parts,
    square_own,
    square_in,
    w_send,
    w_recv,
    b_send,
    b_recv,
    y_send,
    y_recv,
    c_send,
    c_recv,
    sum_send,
    sum_recv,
    back_send,
    back_recv,
    tp_send,
    tp_recv,
    local_sem,
):
    me, column = lax.axis_index("fs"), lax.axis_index("tp")
    rank, width = qm.shape
    far, core = column // 2, lax.rem(column, 2)
    fars = tp // 2
    own_bases = (pair_all.at[me, far, core], ob_all.at[me, far, core])
    pair_rows, ob_rows = pair_all.shape[3], ob_all.shape[3]
    pair_from = aligned(column * pair_rows, pair_rows)
    ob_from = aligned(column * ob_rows, ob_rows)
    loads = [
        pltpu.make_async_copy(source, target, local_sem.at[i])
        for i, (source, target) in enumerate(
            (
                (qb_hbm.at[pair_from, :], pair_all.at[me, far, core, :, pl.ds(0, rank)]),
                (vb_hbm.at[pair_from, :], pair_all.at[me, far, core, :, pl.ds(rank, rank)]),
                (ob_hbm.at[ob_from, :], own_bases[1]),
                (qw_hbm, qw),
                (vw_hbm, vw),
                (ow_hbm, ow),
                (mixer_hbm, mixer),
                (cell_hbm, cell),
                (qg_hbm, qg),
                (vg_hbm, vg),
                (og_hbm, og),
            )
        )
    ]
    for load in loads:
        load.start()

    barrier = pltpu.get_barrier_semaphore()
    for k in range(1, fs):
        pl.semaphore_signal(
            barrier, inc=1, device_id={"fs": lax.rem(me + k, fs)}, device_id_type=MESH
        )
    for k in range(1, tp):
        pl.semaphore_signal(
            barrier, inc=1, device_id={"tp": lax.rem(column + k, tp)}, device_id_type=MESH
        )
    pl.semaphore_wait(barrier, fs + tp - 2)

    for load in loads[:3]:
        load.wait()
    bases = (pair_all, ob_all)
    sent = []
    for k in range(1, fs):
        for n, whole in enumerate(bases):
            mine = whole.at[me, far, core]
            copy = remote(
                mine,
                mine,
                b_send.at[n, k - 1],
                b_recv.at[n, k - 1],
                fs=lax.rem(me + k, fs),
            )
            copy.start()
            sent.append(copy)

    for load in loads[3:6]:
        load.wait()
    wholes = (qw_all, vw_all, ow_all)
    for own, whole in zip((qw, vw, ow), wholes):
        block = own.shape[0]
        whole[aligned(me * block, block), :] = own[...].astype(jnp.bfloat16)
    weights = Weights(wholes, fs, me, w_send, w_recv)
    weights.start()
    part[...] = jnp.zeros_like(part)

    for k in range(1, fs):
        source = lax.rem(me + fs - k, fs)
        for n, whole in enumerate(bases):
            there = whole.at[source, far, core]
            remote(
                there,
                there,
                b_send.at[n, k - 1],
                b_recv.at[n, k - 1],
                fs=lax.rem(me + k, fs),
            ).wait_recv()
    for k in range(1, fars):
        for n, whole in enumerate(bases):
            mine = whole.at[:, far, core]
            copy = remote(
                mine,
                mine,
                y_send.at[n, k - 1],
                y_recv.at[n, k - 1],
                tp=lax.rem(far + k, fars) * 2 + core,
            )
            copy.start()
            sent.append(copy)
    for k in range(1, fars):
        source = lax.rem(far + fars - k, fars)
        for n, whole in enumerate(bases):
            there = whole.at[:, source, core]
            remote(
                there,
                there,
                y_send.at[n, k - 1],
                y_recv.at[n, k - 1],
                tp=lax.rem(far + k, fars) * 2 + core,
            ).wait_recv()
    for n, whole in enumerate(bases):
        mine = whole.at[:, :, core]
        copy = remote(mine, mine, c_send.at[n], c_recv.at[n], tp=far * 2 + 1 - core)
        copy.start()
        sent.append(copy)
    for load in loads[6:]:
        load.wait()
    for n, whole in enumerate(bases):
        there = whole.at[:, :, 1 - core]
        remote(there, there, c_send.at[n], c_recv.at[n], tp=far * 2 + 1 - core).wait_recv()

    tile = 256

    def project(rows, grad):
        turned = jnp.transpose(rows)
        high = turned.astype(jnp.bfloat16)
        low = (turned - high.astype(jnp.float32)).astype(jnp.bfloat16)
        both = matmul(jnp.concatenate([high, low], axis=0), grad)
        return both[:rank] + both[rank:]

    def flat(ref):
        value = ref[...]
        return value.reshape(-1, value.shape[-1])

    def step(t, carry):
        at = aligned(t * tile, tile)
        rows = matmul(mixer[at, :], flat(pair_all))
        part[:, :width] += project(rows[:, :rank], qg[at, :])
        part[:, width : 2 * width] += project(rows[:, rank:], vg[at, :])
        part[:, 2 * width :] += project(matmul(cell[at, :], flat(ob_all)), og[at, :])
        return carry

    lax.fori_loop(0, mixer.shape[0] // tile, step, 0)

    first_owner = (fs - owners) // 2
    share = rank // owners

    def owns(index):
        return (index >= first_owner) & (index < first_owner + owners)

    def strip_of(index):
        return lax.rem(index - first_owner + fs, owners)

    def strip(index):
        return aligned(strip_of(index) * share, share)

    drains = []
    for k in range(1, fs):
        target = lax.rem(me + k, fs)
        copy = remote(
            part.at[strip(target), :],
            parts.at[k - 1],
            sum_send.at[k - 1],
            sum_recv.at[k - 1],
            fs=target,
        )
        pl.when(owns(target))(copy.start)
        drains.append((copy, owns(target)))

    weights.relay(1)

    def gram(ref):
        rows, size = ref.shape[3], ref.shape[4]

        def add(i, total):
            piece = ref[i].reshape(-1, size)
            turned = jnp.transpose(piece.astype(jnp.float32)).astype(jnp.bfloat16)
            return total + matmul(turned, piece)

        return lax.fori_loop(0, ref.shape[0], add, jnp.zeros((size, size), jnp.float32))

    gram_pair = gram(pair_all)
    gram_output = gram(ob_all)

    back = []
    for k in range(1, fs):
        target = lax.rem(me + k, fs)
        mine = proj.at[strip(me), :]
        back.append(
            remote(mine, mine, back_send.at[k - 1], back_recv.at[k - 1], fs=target)
        )

    @pl.when(owns(me))
    def _():
        for k in range(1, fs):
            remote(
                part.at[strip(me), :],
                parts.at[k - 1],
                sum_send.at[k - 1],
                sum_recv.at[k - 1],
                fs=lax.rem(me + k, fs),
            ).wait_recv()
        total = part[strip(me), :]
        for k in range(1, fs):
            total = total + parts[k - 1]
        proj[strip(me), :] = total.astype(proj.dtype)
        for copy in back:
            copy.start()

    weights.relay(2)
    weights.relay_cross()

    for k in range(1, fs):
        source = lax.rem(me + fs - k, fs)
        there = proj.at[strip(source), :]
        copy = remote(
            there, there, back_send.at[k - 1], back_recv.at[k - 1], fs=lax.rem(me + k, fs)
        )
        pl.when(owns(source))(copy.wait_recv)

    def norm(basis_gram, projected, mean, square):
        direction = moments(projected.astype(jnp.float32), mean[...], square[...])[2]
        turned = jnp.dot(
            basis_gram,
            direction,
            precision=lax.Precision.HIGHEST,
            preferred_element_type=jnp.float32,
        )
        lanes = jnp.sum(direction * turned, axis=0, keepdims=True)
        return jnp.sum(lanes, axis=1, keepdims=True)

    partial = (
        norm(gram_pair[:rank, :rank], proj[:, :width], qm, qs)
        + norm(gram_pair[rank:, rank:], proj[:, width : 2 * width], vm, vs)
        + norm(gram_output, proj[:, 2 * width :], om, os)
    )
    square_own[...] = jnp.broadcast_to(partial, square_own.shape)
    shares = []
    for k in range(1, tp):
        copy = remote(
            square_own,
            square_in.at[k - 1],
            tp_send.at[k - 1],
            tp_recv.at[k - 1],
            tp=lax.rem(column + k, tp),
        )
        copy.start()
        shares.append(copy)

    weights.relay(3)
    for copy in shares:
        copy.wait_recv()
    whole_squares = square_own[...]
    for k in range(1, tp):
        whole_squares = whole_squares + square_in[k - 1]
    squares[...] = whole_squares
    weights.finish()
    for copy in sent + shares:
        copy.wait_send()
    for copy, inside in drains:
        pl.when(inside)(copy.wait_send)

    @pl.when(owns(me))
    def _():
        for copy in back:
            copy.wait_send()


def exchange(fs, tp, mixer, cell, grads, bases, weights, means, olds):
    rank = means[0].shape[0]
    total = sum(grad.shape[1] for grad in grads)
    owners = min(4, fs)
    bf16, f32 = jnp.bfloat16, jnp.float32
    hbm, vmem = pl.BlockSpec(memory_space=pl.ANY), pl.BlockSpec(memory_space=pltpu.VMEM)
    dma = pltpu.SemaphoreType.DMA

    def whole(array):
        return jax.ShapeDtypeStruct((array.shape[0] * fs, array.shape[1]), bf16)

    def parted(array, columns):
        return jax.ShapeDtypeStruct((fs, tp // 2, 2, array.shape[0] // tp, columns), bf16)

    return pl.pallas_call(
        functools.partial(kernel, fs, tp, owners),
        out_shape=(
            *(whole(weight) for weight in weights),
            parted(bases[0], 2 * rank),
            parted(bases[2], rank),
            jax.ShapeDtypeStruct((rank, total), bf16),
            jax.ShapeDtypeStruct((8, 128), f32),
        ),
        in_specs=[hbm] * 11 + [vmem] * 6,
        out_specs=(vmem,) * 7,
        scratch_shapes=[
            *(pltpu.VMEM(array.shape, bf16) for array in (mixer, cell, *grads)),
            *(pltpu.VMEM(array.shape, f32) for array in weights),
            pltpu.VMEM((rank, total), f32),
            pltpu.VMEM((fs - 1, rank // owners, total), f32),
            pltpu.VMEM((8, 128), f32),
            pltpu.VMEM((tp - 1, 8, 128), f32),
            dma((3, CHUNKS, max(15, fs - 1))),
            dma((3, CHUNKS, max(13, fs - 1))),
            dma((2, fs - 1)),
            dma((2, fs - 1)),
            dma((2, max(1, tp // 2 - 1))),
            dma((2, max(1, tp // 2 - 1))),
            dma((2,)),
            dma((2,)),
            dma((fs - 1,)),
            dma((fs - 1,)),
            dma((fs - 1,)),
            dma((fs - 1,)),
            dma((tp - 1,)),
            dma((tp - 1,)),
            dma((11,)),
        ],
        compiler_params=pltpu.CompilerParams(
            collective_id=0, has_side_effects=True, vmem_limit_bytes=VMEM_MAIN
        ),
    )(mixer, cell, *grads, *bases, *weights, *means, *olds)


VMEM_MAIN = 28 * 1024 * 1024
VMEM_LAST = 24 * 1024 * 1024


def last_kernel(entries, *refs):
    inputs, outputs, scratch = refs[:13], refs[13:25], refs[25:]
    wholes, pair, ob, proj, squares = inputs[0:3], inputs[3], inputs[4], inputs[5], inputs[6]
    means, olds = inputs[7:10], inputs[10:13]
    stage, sem = scratch[:12], scratch[12]
    rank, width = means[0].shape
    me = lax.axis_index("fs")
    factor = 1.0 / jnp.sqrt(squares[0:1, 0:1] / entries + floor_mean)
    copies = []

    def put(index, source, target):
        copy = pltpu.make_async_copy(source, target, sem.at[len(copies)])
        copy.start()
        copies.append(copy)

    bases = ((pair, 0), (pair, rank), (ob, 0))
    lefts = (0, width, 2 * width)
    for n in range(3):
        columns = means[n].shape[1]
        projected = proj[:, lefts[n] : lefts[n] + columns].astype(jnp.float32)
        first, second, direction = moments(projected, means[n][...], olds[n][...])
        stage[6 + n][...] = first
        stage[9 + n][...] = second
        put(6 + n, stage[6 + n], outputs[6 + n])
        put(9 + n, stage[9 + n], outputs[9 + n])
        high = direction.astype(jnp.bfloat16)
        low = (direction - high.astype(jnp.float32)).astype(jnp.bfloat16)
        both = jnp.concatenate([high, low], axis=0)
        base, left = bases[n]
        blocks = wholes[n].shape[0] // base.shape[0]
        own = base[me, :, left : left + rank]
        stage[n][...] = -factor * matmul(jnp.concatenate([own, own], axis=1), both)
        put(n, stage[n], outputs[n])
        scale = (-learn_rate) * factor
        for o in range(base.shape[0]):
            rows = pl.ds(o * blocks, blocks)
            piece = base[o, :, left : left + rank]
            update = matmul(piece, high)
            stage[3 + n][rows, :] = (
                wholes[n][rows, :].astype(jnp.float32) + scale * update
            ).astype(jnp.bfloat16)
            put(3 + n, stage[3 + n].at[rows, :], outputs[3 + n].at[rows, :])
    for copy in copies:
        copy.wait()


def body(fs, tp):
    def local(
        mixer_input,
        cell_output,
        query_grad,
        value_grad,
        output_grad,
        query_weight,
        value_weight,
        output_weight,
        query_basis,
        value_basis,
        output_basis,
        query_mean,
        value_mean,
        output_mean,
        query_square,
        value_square,
        output_square,
    ):
        means = (query_mean, value_mean, output_mean)
        olds = (query_square, value_square, output_square)
        weights = (query_weight, value_weight, output_weight)
        *wholes, pair, ob, proj, squares = exchange(
            fs,
            tp,
            mixer_input,
            cell_output,
            (query_grad, value_grad, output_grad),
            (query_basis, value_basis, output_basis),
            weights,
            means,
            olds,
        )
        entries = float(sum(w.shape[0] * fs * w.shape[1] * tp for w in weights))
        pair = pair.reshape(fs, -1, pair.shape[-1])
        ob = ob.reshape(fs, -1, ob.shape[-1])
        f32 = jnp.float32
        shapes = (
            *(jax.ShapeDtypeStruct(w.shape, f32) for w in weights),
            *(jax.ShapeDtypeStruct(w.shape, w.dtype) for w in wholes),
            *(jax.ShapeDtypeStruct(m.shape, f32) for m in means),
            *(jax.ShapeDtypeStruct(m.shape, f32) for m in olds),
        )
        vmem = pl.BlockSpec(memory_space=pltpu.VMEM)
        return pl.pallas_call(
            functools.partial(last_kernel, entries),
            out_shape=shapes,
            in_specs=[vmem] * 13,
            out_specs=(pl.BlockSpec(memory_space=pl.ANY),) * 12,
            scratch_shapes=[
                *(pltpu.VMEM(s.shape, s.dtype) for s in shapes),
                pltpu.SemaphoreType.DMA((9 + 3 * fs,)),
            ],
            compiler_params=pltpu.CompilerParams(vmem_limit_bytes=VMEM_LAST),
        )(*wholes, pair, ob, proj, squares, *means, *olds)

    return local


def solution(mesh):
    rows, split_both, columns = P("fs", None), P("fs", "tp"), P(None, "tp")
    in_specs = (rows,) * 2 + (split_both,) * 6 + (rows,) * 3 + (columns,) * 6
    out_specs = (split_both,) * 3 + (columns,) * 9
    return jax.shard_map(
        body(mesh.shape["fs"], mesh.shape["tp"]),
        mesh=mesh,
        in_specs=in_specs,
        out_specs=out_specs,
        check_vma=False,
    )
```

time: 216 us -> 188 us (0.87)
  the two profiles are of different devices: /device:TPU:0 before, /device:TPU:24 now
where the time goes in v1:
time: 188 us; the launch traced here: 187 us
  Pallas kernels  170 us (90%)
  local copies, waits for them, and re-layouts  16.2 us (9%)
    pallas_call x1, Pallas kernels, exchange(): pl.pallas_call(functools.partial(kernel, fs, tp, owners), out_shape=(*(wh...  164 us
    unnamed x30, local copies, waits for them, and re-layouts  16.2 us
    pallas_call x1, Pallas kernels, local(): pl.pallas_call(functools.partial(last_kernel, entries), out_shape=shapes,...  6.7 us

profile of v1, /device:TPU:24, one launch (start us, length us, event | category | flops | bytes accessed | tf_op | source)
XLA Modules:
  0.0 187.2 jit_solution(1982858574845118335)
XLA Ops:
  0.7 0.0 copy-start
  0.7 1.0 copy-done
  1.7 0.0 copy-start.1
  1.7 1.0 copy-done.1
  2.7 0.0 copy-start.2
  2.7 1.6 copy-done.2
  4.3 0.0 copy-start.3
  4.3 0.9 copy-done.3
  5.3 0.0 copy-start.4
  5.3 0.9 copy-done.4
  6.2 0.0 copy-start.5
  6.2 0.9 copy-done.5
  7.2 0.0 copy-start.6
  7.2 0.9 copy-done.6
  8.1 0.0 copy-start.7
  8.1 1.2 copy-done.7
  9.4 0.0 copy-start.8
  9.4 1.2 copy-done.8
  10.6 0.0 copy-start.9
  10.6 1.2 copy-done.9
  11.8 0.0 copy-start.10
  11.8 1.2 copy-done.10
  13.0 0.0 copy-start.11
  13.0 1.2 copy-done.11
  14.3 0.0 copy-start.12
  14.3 0.9 copy-done.12
  15.2 0.0 copy-start.13
  15.2 0.9 copy-done.13
  16.1 0.0 copy-start.14
  16.1 0.8 copy-done.14
  16.9 163.6 %shard_map.256 = (bf16[4096,512]{1,0:T(8,128)(2,1)S(1)}, bf16[4096,512]{1,0:T(8,128)(2,1)S(1)}, bf16[2048,1024]{1,0:T(8,128)(2,1)S(1)}, bf16[8,2,2,128,256]{4,3,...) custom-call(bf16[1024,4096]{1,0:T(8,128)(2,1)} %mixer_hbm.1, ...), custom_call_target="tpu_custom_call" | custom-call | tf_op jit(solution)/shard_map/pallas_call | solution.py:511
  180.5 6.7 %shard_map.257 = (f32[512,512]{1,0:T(8,128)}, f32[512,512]{1,0:T(8,128)}, f32[256,1024]{1,0:T(8,128)}, bf16[4096,512]{1,0:T(8,128)(2,1)}, bf16[4096,512]{1,0:T(8...) custom-call(bf16[4096,512]{1,0:T(8,128)(2,1)S(1)} %get-tuple-element, ...), custom_call_target="tpu_custom_call" | custom-call | tf_op jit(solution)/shard_map/pallas_call | solution.py:646
Async XLA Ops:
  0.7 1.0 copy-start
  1.7 1.0 copy-start.1
  2.7 1.6 copy-start.2
  4.3 0.9 copy-start.3
  5.3 0.9 copy-start.4
  6.2 0.9 copy-start.5
  7.2 0.9 copy-start.6
  8.1 1.2 copy-start.7
  9.4 1.2 copy-start.8
  10.6 1.2 copy-start.9
  11.8 1.2 copy-start.10
  13.0 1.2 copy-start.11
  14.3 0.9 copy-start.12
  15.2 0.9 copy-start.13
  16.1 0.8 copy-start.14

commit v2 on v1

--- a/solution.py
+++ b/solution.py
@@ -194,18 +194,20 @@
     qw_hbm,
     vw_hbm,
     ow_hbm,
-    qm,
-    vm,
-    om,
-    qs,
-    vs,
-    os,
+    qm_hbm,
+    vm_hbm,
+    om_hbm,
+    qs_hbm,
+    vs_hbm,
+    os_hbm,
     qw_all,
     vw_all,
     ow_all,
     pair_all,
     ob_all,
-    proj,
+    firsts,
+    seconds,
+    dirs,
     squares,
     mixer,
     cell,
@@ -215,6 +217,9 @@
     qw,
     vw,
     ow,
+    means,
+    olds,
+    proj,
     part,
     parts,
     square_own,
@@ -236,7 +241,7 @@
     local_sem,
 ):
     me, column = lax.axis_index("fs"), lax.axis_index("tp")
-    rank, width = qm.shape
+    rank, width = qm_hbm.shape
     far, core = column // 2, lax.rem(column, 2)
     fars = tp // 2
     own_bases = (pair_all.at[me, far, core], ob_all.at[me, far, core])
@@ -258,6 +263,12 @@
                 (qg_hbm, qg),
                 (vg_hbm, vg),
                 (og_hbm, og),
+                (qm_hbm, means.at[:, pl.ds(0, width)]),
+                (vm_hbm, means.at[:, pl.ds(width, width)]),
+                (om_hbm, means.at[:, pl.ds(2 * width, 2 * width)]),
+                (qs_hbm, olds.at[:, pl.ds(0, width)]),
+                (vs_hbm, olds.at[:, pl.ds(width, width)]),
+                (os_hbm, olds.at[:, pl.ds(2 * width, 2 * width)]),
             )
         )
     ]
@@ -437,6 +448,7 @@
 
     weights.relay(2)
     weights.relay_cross()
+    weights.relay(3)
 
     for k in range(1, fs):
         source = lax.rem(me + fs - k, fs)
@@ -446,8 +458,16 @@
         )
         pl.when(owns(source))(copy.wait_recv)
 
-    def norm(basis_gram, projected, mean, square):
-        direction = moments(projected.astype(jnp.float32), mean[...], square[...])[2]
+    def norm(basis_gram, left, columns):
+        at = pl.ds(left, columns)
+        first, second, direction = moments(
+            proj[:, at].astype(jnp.float32), means[:, at], olds[:, at]
+        )
+        firsts[:, at] = first
+        seconds[:, at] = second
+        high = direction.astype(jnp.bfloat16)
+        dirs[:rank, at] = high
+        dirs[rank:, at] = (direction - high.astype(jnp.float32)).astype(jnp.bfloat16)
         turned = jnp.dot(
             basis_gram,
             direction,
@@ -458,9 +478,9 @@
         return jnp.sum(lanes, axis=1, keepdims=True)
 
     partial = (
-        norm(gram_pair[:rank, :rank], proj[:, :width], qm, qs)
-        + norm(gram_pair[rank:, rank:], proj[:, width : 2 * width], vm, vs)
-        + norm(gram_output, proj[:, 2 * width :], om, os)
+        norm(gram_pair[:rank, :rank], 0, width)
+        + norm(gram_pair[rank:, rank:], width, width)
+        + norm(gram_output, 2 * width, 2 * width)
     )
     square_own[...] = jnp.broadcast_to(partial, square_own.shape)
     shares = []
@@ -475,7 +495,6 @@
         copy.start()
         shares.append(copy)
 
-    weights.relay(3)
     for copy in shares:
         copy.wait_recv()
     whole_squares = square_own[...]
@@ -499,7 +518,7 @@
     total = sum(grad.shape[1] for grad in grads)
     owners = min(4, fs)
     bf16, f32 = jnp.bfloat16, jnp.float32
-    hbm, vmem = pl.BlockSpec(memory_space=pl.ANY), pl.BlockSpec(memory_space=pltpu.VMEM)
+    hbm, vmem = pl.BlockSpec(memory_space=pltpu.HBM), pl.BlockSpec(memory_space=pltpu.VMEM)
     dma = pltpu.SemaphoreType.DMA
 
     def whole(array):
@@ -514,14 +533,19 @@
             *(whole(weight) for weight in weights),
             parted(bases[0], 2 * rank),
             parted(bases[2], rank),
-            jax.ShapeDtypeStruct((rank, total), bf16),
+            jax.ShapeDtypeStruct((rank, total), f32),
+            jax.ShapeDtypeStruct((rank, total), f32),
+            jax.ShapeDtypeStruct((2 * rank, total), bf16),
             jax.ShapeDtypeStruct((8, 128), f32),
         ),
-        in_specs=[hbm] * 11 + [vmem] * 6,
-        out_specs=(vmem,) * 7,
+        in_specs=[hbm] * 17,
+        out_specs=(vmem,) * 9,
         scratch_shapes=[
             *(pltpu.VMEM(array.shape, bf16) for array in (mixer, cell, *grads)),
             *(pltpu.VMEM(array.shape, f32) for array in weights),
+            pltpu.VMEM((rank, total), f32),
+            pltpu.VMEM((rank, total), f32),
+            pltpu.VMEM((rank, total), bf16),
             pltpu.VMEM((rank, total), f32),
             pltpu.VMEM((fs - 1, rank // owners, total), f32),
             pltpu.VMEM((8, 128), f32),
@@ -540,60 +564,54 @@
             dma((fs - 1,)),
             dma((tp - 1,)),
             dma((tp - 1,)),
-            dma((11,)),
+            dma((17,)),
         ],
         compiler_params=pltpu.CompilerParams(
             collective_id=0, has_side_effects=True, vmem_limit_bytes=VMEM_MAIN
         ),
-    )(mixer, cell, *grads, *bases, *weights, *means, *olds)
-
-
-VMEM_MAIN = 28 * 1024 * 1024
+    )(*(pltpu.with_memory_space_constraint(a, pltpu.HBM) for a in (mixer, cell, *grads, *bases, *weights, *means, *olds)))
+
+
+VMEM_MAIN = 30 * 1024 * 1024
 VMEM_LAST = 24 * 1024 * 1024
 
 
 def last_kernel(entries, *refs):
-    inputs, outputs, scratch = refs[:13], refs[13:25], refs[25:]
-    wholes, pair, ob, proj, squares = inputs[0:3], inputs[3], inputs[4], inputs[5], inputs[6]
-    means, olds = inputs[7:10], inputs[10:13]
-    stage, sem = scratch[:12], scratch[12]
-    rank, width = means[0].shape
+    wholes, (pair, ob, firsts, seconds, dirs, squares) = refs[:3], refs[3:9]
+    outputs, stage, sem = refs[9:21], refs[21:27], refs[27]
+    rank = pair.shape[2] // 2
     me = lax.axis_index("fs")
-    factor = 1.0 / jnp.sqrt(squares[0:1, 0:1] / entries + floor_mean)
     copies = []
 
-    def put(index, source, target):
+    def put(source, target):
         copy = pltpu.make_async_copy(source, target, sem.at[len(copies)])
         copy.start()
         copies.append(copy)
 
+    cuts, left = [], 0
+    for whole in wholes:
+        cuts.append(pl.ds(left, whole.shape[1]))
+        left += whole.shape[1]
+    for n, cut in enumerate(cuts):
+        put(firsts.at[:, cut], outputs[6 + n])
+        put(seconds.at[:, cut], outputs[9 + n])
+    factor = 1.0 / jnp.sqrt(squares[0:1, 0:1] / entries + floor_mean)
+    scale = -learn_rate * factor
     bases = ((pair, 0), (pair, rank), (ob, 0))
-    lefts = (0, width, 2 * width)
-    for n in range(3):
-        columns = means[n].shape[1]
-        projected = proj[:, lefts[n] : lefts[n] + columns].astype(jnp.float32)
-        first, second, direction = moments(projected, means[n][...], olds[n][...])
-        stage[6 + n][...] = first
-        stage[9 + n][...] = second
-        put(6 + n, stage[6 + n], outputs[6 + n])
-        put(9 + n, stage[9 + n], outputs[9 + n])
-        high = direction.astype(jnp.bfloat16)
-        low = (direction - high.astype(jnp.float32)).astype(jnp.bfloat16)
-        both = jnp.concatenate([high, low], axis=0)
-        base, left = bases[n]
-        blocks = wholes[n].shape[0] // base.shape[0]
-        own = base[me, :, left : left + rank]
+    for n, (cut, (base, low)) in enumerate(zip(cuts, bases)):
+        both = dirs[:, cut]
+        own = base[me, :, low : low + rank]
         stage[n][...] = -factor * matmul(jnp.concatenate([own, own], axis=1), both)
-        put(n, stage[n], outputs[n])
-        scale = (-learn_rate) * factor
+        put(stage[n], outputs[n])
+        high = both[:rank]
+        block = base.shape[1]
         for o in range(base.shape[0]):
-            rows = pl.ds(o * blocks, blocks)
-            piece = base[o, :, left : left + rank]
-            update = matmul(piece, high)
+            rows = pl.ds(o * block, block)
+            update = matmul(base[o, :, low : low + rank], high)
             stage[3 + n][rows, :] = (
                 wholes[n][rows, :].astype(jnp.float32) + scale * update
             ).astype(jnp.bfloat16)
-            put(3 + n, stage[3 + n].at[rows, :], outputs[3 + n].at[rows, :])
+            put(stage[3 + n].at[rows, :], outputs[3 + n].at[rows, :])
     for copy in copies:
         copy.wait()
 
@@ -621,7 +639,7 @@
         means = (query_mean, value_mean, output_mean)
         olds = (query_square, value_square, output_square)
         weights = (query_weight, value_weight, output_weight)
-        *wholes, pair, ob, proj, squares = exchange(
+        *wholes, pair, ob, firsts, seconds, dirs, squares = exchange(
             fs,
             tp,
             mixer_input,
@@ -646,14 +664,14 @@
         return pl.pallas_call(
             functools.partial(last_kernel, entries),
             out_shape=shapes,
-            in_specs=[vmem] * 13,
+            in_specs=[vmem] * 9,
             out_specs=(pl.BlockSpec(memory_space=pl.ANY),) * 12,
             scratch_shapes=[
-                *(pltpu.VMEM(s.shape, s.dtype) for s in shapes),
+                *(pltpu.VMEM(s.shape, s.dtype) for s in shapes[:6]),
                 pltpu.SemaphoreType.DMA((9 + 3 * fs,)),
             ],
             compiler_params=pltpu.CompilerParams(vmem_limit_bytes=VMEM_LAST),
-        )(*wholes, pair, ob, proj, squares, *means, *olds)
+        )(*wholes, pair, ob, firsts, seconds, dirs, squares)
 
     return local
 

time: 188 us -> 156 us (0.83)
  the two profiles are of different devices: /device:TPU:24 before, /device:TPU:0 now
where the time goes in v2:
time: 156 us
  Pallas kernels  155 us (99%)
    pallas_call x1, Pallas kernels, exchange(): pl.pallas_call(functools.partial(kernel, fs, tp, owners), out_shape=(*(wh...  148 us
    pallas_call x1, Pallas kernels, local(): pl.pallas_call(functools.partial(last_kernel, entries), out_shape=shapes,...  6.71 us

profile of v2, /device:TPU:0, one launch (start us, length us, event | category | flops | bytes accessed | tf_op | source)
XLA Modules:
  0.0 155.6 jit_solution(16537455340324495567)
XLA Ops:
  0.7 148.2 %shard_map.256 = (bf16[4096,512]{1,0:T(8,128)(2,1)S(1)}, bf16[4096,512]{1,0:T(8,128)(2,1)S(1)}, bf16[2048,1024]{1,0:T(8,128)(2,1)S(1)}, bf16[8,2,2,128,256]{4,3,...) custom-call(bf16[1024,4096]{1,0:T(8,128)(2,1)} %mixer_hbm.1, ...), custom_call_target="tpu_custom_call" | custom-call | tf_op jit(solution)/shard_map/pallas_call | solution.py:530
  148.9 6.7 %shard_map.257 = (f32[512,512]{1,0:T(8,128)}, f32[512,512]{1,0:T(8,128)}, f32[256,1024]{1,0:T(8,128)}, bf16[4096,512]{1,0:T(8,128)(2,1)}, bf16[4096,512]{1,0:T(8...) custom-call(bf16[4096,512]{1,0:T(8,128)(2,1)S(1)} %get-tuple-element, ...), custom_call_target="tpu_custom_call" | custom-call | tf_op jit(solution)/shard_map/pallas_call | solution.py:664

commit v3 on v2

--- a/solution.py
+++ b/solution.py
@@ -13,7 +13,8 @@
 learn_rate = 0.05
 
 MESH = pl.DeviceIdType.MESH
-LINE_CHUNKS = 5
+LINE_CHUNKS = 7
+BASE_LINE = (False, True)
 CHUNKS = 4
 
 
@@ -31,9 +32,10 @@
     return pl.ds(pl.multiple_of(start, size), size)
 
 
-class Weights:
-    def __init__(self, wholes, fs, me, send_sem, recv_sem):
-        self.wholes, self.fs, self.me = wholes, fs, me
+class Gather:
+    def __init__(self, fs, me, count, chunks, slot, line, send_sem, recv_sem):
+        self.fs, self.me, self.count, self.chunks = fs, me, count, chunks
+        self.slot, self.line = slot, line
         self.send_sem, self.recv_sem = send_sem, recv_sem
         self.relayed = fs == 8
         self.place, self.side = me // 2, lax.rem(me, 2)
@@ -41,12 +43,6 @@
     def index(self, step, other=False):
         place = lax.rem(self.place + step + 4, 4)
         return place * 2 + (1 - self.side if other else self.side)
-
-    def slot(self, w, i, origin):
-        whole = self.wholes[w]
-        block = whole.shape[0] // self.fs
-        rows = block // CHUNKS
-        return whole.at[aligned(origin * block + i * rows, rows), :]
 
     def copy(self, w, i, origin, site, role, target):
         return pltpu.make_async_remote_copy(
@@ -58,7 +54,7 @@
             device_id_type=MESH,
         )
 
-    def arrive(self, w, i, origin, role, inside):
+    def arrive(self, w, i, origin, role, inside=True):
         copy = self.copy(w, i, origin, 0, role, lax.rem(self.me + 1, self.fs))
         if inside is True:
             copy.wait_recv()
@@ -67,7 +63,7 @@
 
     def sites(self, w, i):
         p = self.place
-        line = i * len(self.wholes) + w < LINE_CHUNKS
+        line = self.line(w, i)
         out = [
             (0, self.me, 0, self.index(1), p < 3),
             (1, self.me, 3, self.index(-1), p > 0),
@@ -88,62 +84,87 @@
         out.append((14, cross, 10, self.index(-1), (p > 0) & (line | (p == 3))))
         return {site[0]: site for site in out}
 
-    def direct(self, w, i):
-        return {
-            k - 1: (k - 1, self.me, k - 1, lax.rem(self.me + k, self.fs), True)
-            for k in range(1, self.fs)
-        }
-
-    def send(self, w, i, *wanted):
+    def direct(self):
+        return [(k - 1, lax.rem(self.me + k, self.fs)) for k in range(1, self.fs)]
+
+    def send(self, w, i, wanted, also=None):
         table = self.sites(w, i)
         for site in wanted:
             number, origin, role, target, inside = table[site]
             copy = self.copy(w, i, origin, number, role, target)
+            if also is not None:
+                inside = inside & also
             if inside is True:
                 copy.start()
             else:
                 pl.when(inside)(copy.start)
 
-    def each(self, step):
+    def each(self, step, low=0, high=None, only=None):
+        high = self.chunks if high is None else high
+
         def chunk(i, carry):
-            for w in range(len(self.wholes)):
+            for w in range(self.count) if only is None else (only,):
                 step(w, i)
             return carry
 
-        lax.fori_loop(0, CHUNKS, chunk, 0)
-
-    def start(self):
+        if high - low == 1:
+            chunk(low, 0)
+        elif high > low:
+            lax.fori_loop(low, high, chunk, 0)
+
+    def start(self, low=0, high=None, only=None):
         def step(w, i):
             if self.relayed:
-                self.send(w, i, 0, 1, 2)
+                self.send(w, i, (0, 1, 2))
             else:
-                for number, origin, role, target, _ in self.direct(w, i).values():
-                    self.copy(w, i, origin, number, role, target).start()
-
-        self.each(step)
-
-    def relay(self, d):
-        if not self.relayed:
-            return
+                for number, target in self.direct():
+                    self.copy(w, i, self.me, number, number, target).start()
+
+        self.each(step, low, high, only)
+
+    def relay_out(self, low=0, high=None):
+        p = self.place
+
+        def step(w, i):
+            self.arrive(w, i, self.index(-1), 0, p >= 2)
+            self.send(w, i, (3, 7), p >= 2)
+            self.arrive(w, i, self.index(1), 3, p <= 1)
+            self.send(w, i, (5, 10), p <= 1)
+
+        if self.relayed:
+            self.each(step, low, high)
+
+    def relay_in(self, low=0, high=None):
+        p = self.place
+
+        def step(w, i):
+            self.arrive(w, i, self.index(-1), 0, p == 1)
+            self.send(w, i, (3,), p == 1)
+            self.arrive(w, i, self.index(1), 3, p == 2)
+            self.send(w, i, (5,), p == 2)
+
+        if self.relayed:
+            self.each(step, low, high)
+
+    def relay(self, d, low=0, high=None):
         p = self.place
 
         def step(w, i):
             self.arrive(w, i, self.index(-d), d - 1, p >= d)
-            self.send(w, i, *((2 + d, 6 + d) if d < 3 else (6 + d,)))
+            self.send(w, i, (2 + d, 6 + d) if d < 3 else (6 + d,))
             self.arrive(w, i, self.index(d), 2 + d, p + d < 4)
-            self.send(w, i, *((4 + d, 9 + d) if d < 3 else (9 + d,)))
-
-        self.each(step)
+            self.send(w, i, (4 + d, 9 + d) if d < 3 else (9 + d,))
+
+        if self.relayed:
+            self.each(step, low, high)
 
     def relay_cross(self):
-        if not self.relayed:
-            return
-
         def step(w, i):
-            self.arrive(w, i, self.index(0, True), 6, True)
-            self.send(w, i, 13, 14)
-
-        self.each(step)
+            self.arrive(w, i, self.index(0, True), 6)
+            self.send(w, i, (13, 14))
+
+        if self.relayed:
+            self.each(step)
 
     def finish(self):
         p = self.place
@@ -151,13 +172,20 @@
         def step(w, i):
             if not self.relayed:
                 for k in range(1, self.fs):
-                    self.arrive(w, i, lax.rem(self.me + self.fs - k, self.fs), k - 1, True)
-                for number, origin, role, target, _ in self.direct(w, i).values():
-                    self.copy(w, i, origin, number, role, target).wait_send()
+                    self.arrive(w, i, lax.rem(self.me + self.fs - k, self.fs), k - 1)
                 return
             for d in (1, 2, 3):
                 self.arrive(w, i, self.index(-d, True), 6 + d, p >= d)
                 self.arrive(w, i, self.index(d, True), 9 + d, p + d < 4)
+
+        self.each(step)
+
+    def drain(self):
+        def step(w, i):
+            if not self.relayed:
+                for number, target in self.direct():
+                    self.copy(w, i, self.me, number, number, target).wait_send()
+                return
             for number, origin, role, target, inside in self.sites(w, i).values():
                 copy = self.copy(w, i, origin, number, role, target)
                 if inside is True:
@@ -236,6 +264,7 @@
     sum_recv,
     back_send,
     back_recv,
+    over_send,
     tp_send,
     tp_recv,
     local_sem,
@@ -289,41 +318,46 @@
     for load in loads[:3]:
         load.wait()
     bases = (pair_all, ob_all)
+    wholes = (qw_all, vw_all, ow_all)
     sent = []
-    for k in range(1, fs):
-        for n, whole in enumerate(bases):
-            mine = whole.at[me, far, core]
-            copy = remote(
-                mine,
-                mine,
-                b_send.at[n, k - 1],
-                b_recv.at[n, k - 1],
-                fs=lax.rem(me + k, fs),
-            )
-            copy.start()
-            sent.append(copy)
-
+
+    def base_slot(w, i, origin):
+        return bases[w].at[origin, far, core]
+
+    def weight_slot(w, i, origin):
+        block = wholes[w].shape[0] // fs
+        rows = block // CHUNKS
+        return wholes[w].at[aligned(origin * block + i * rows, rows), :]
+
+    parts_of_bases = Gather(
+        fs, me, 2, 1, base_slot, lambda w, i: BASE_LINE[w], b_send, b_recv
+    )
+    weights = Gather(
+        fs,
+        me,
+        3,
+        CHUNKS,
+        weight_slot,
+        lambda w, i: i * len(wholes) + w < LINE_CHUNKS,
+        w_send,
+        w_recv,
+    )
+    parts_of_bases.start()
     for load in loads[3:6]:
         load.wait()
-    wholes = (qw_all, vw_all, ow_all)
     for own, whole in zip((qw, vw, ow), wholes):
         block = own.shape[0]
         whole[aligned(me * block, block), :] = own[...].astype(jnp.bfloat16)
-    weights = Weights(wholes, fs, me, w_send, w_recv)
-    weights.start()
+    weights.start(0, 1, 0)
     part[...] = jnp.zeros_like(part)
-
-    for k in range(1, fs):
-        source = lax.rem(me + fs - k, fs)
-        for n, whole in enumerate(bases):
-            there = whole.at[source, far, core]
-            remote(
-                there,
-                there,
-                b_send.at[n, k - 1],
-                b_recv.at[n, k - 1],
-                fs=lax.rem(me + k, fs),
-            ).wait_recv()
+    parts_of_bases.relay(1)
+    parts_of_bases.relay_cross()
+    weights.start(0, 1, 1)
+    parts_of_bases.relay(2)
+    weights.start(0, 1, 2)
+    parts_of_bases.relay(3)
+    weights.start(1)
+    parts_of_bases.finish()
     for k in range(1, fars):
         for n, whole in enumerate(bases):
             mine = whole.at[:, far, core]
@@ -336,6 +370,7 @@
             )
             copy.start()
             sent.append(copy)
+    weights.relay_out(0, 2)
     for k in range(1, fars):
         source = lax.rem(far + fars - k, fars)
         for n, whole in enumerate(bases):
@@ -406,7 +441,8 @@
         pl.when(owns(target))(copy.start)
         drains.append((copy, owns(target)))
 
-    weights.relay(1)
+    weights.relay_out(2)
+    weights.relay_in(0, 1)
 
     def gram(ref):
         rows, size = ref.shape[3], ref.shape[4]
@@ -421,13 +457,30 @@
     gram_pair = gram(pair_all)
     gram_output = gram(ob_all)
 
+    side = lax.rem(me, 2)
+    relayed = weights.relayed
     back = []
     for k in range(1, fs):
         target = lax.rem(me + k, fs)
         mine = proj.at[strip(me), :]
-        back.append(
-            remote(mine, mine, back_send.at[k - 1], back_recv.at[k - 1], fs=target)
-        )
+        inside = owns(me)
+        if relayed:
+            inside = inside & (owns(target) | (lax.rem(target, 2) == side))
+        copy = remote(
+            mine, mine, back_send.at[k - 1], back_recv.at[strip_of(me)], fs=target
+        )
+        back.append((copy, inside))
+    other = me + 1 - 2 * side if relayed else lax.rem(me + 1, fs)
+    returned = []
+    for j in range(owners):
+        there = proj.at[pl.ds(j * share, share), :]
+        source = first_owner + j
+        straight = me != source
+        if relayed:
+            same = side == source % 2
+            straight = straight & (owns(me) | same)
+        over = remote(there, there, over_send.at[j], back_recv.at[j], fs=other)
+        returned.append((over, straight, jnp.logical_not(owns(me)) if relayed else None, source % 2))
 
     @pl.when(owns(me))
     def _():
@@ -443,20 +496,22 @@
         for k in range(1, fs):
             total = total + parts[k - 1]
         proj[strip(me), :] = total.astype(proj.dtype)
-        for copy in back:
-            copy.start()
-
+
+    for copy, inside in back:
+        pl.when(inside)(copy.start)
+
+    weights.relay_in(1)
     weights.relay(2)
     weights.relay_cross()
+
+    for over, straight, at_end, parity in returned:
+        pl.when(straight)(over.wait_recv)
+        if relayed:
+            pl.when(at_end & (side == parity))(over.start)
     weights.relay(3)
-
-    for k in range(1, fs):
-        source = lax.rem(me + fs - k, fs)
-        there = proj.at[strip(source), :]
-        copy = remote(
-            there, there, back_send.at[k - 1], back_recv.at[k - 1], fs=lax.rem(me + k, fs)
-        )
-        pl.when(owns(source))(copy.wait_recv)
+    if relayed:
+        for over, straight, at_end, parity in returned:
+            pl.when(at_end & (side != parity))(over.wait_recv)
 
     def norm(basis_gram, left, columns):
         at = pl.ds(left, columns)
@@ -504,13 +559,13 @@
     weights.finish()
     for copy in sent + shares:
         copy.wait_send()
-    for copy, inside in drains:
+    for copy, inside in drains + back:
         pl.when(inside)(copy.wait_send)
-
-    @pl.when(owns(me))
-    def _():
-        for copy in back:
-            copy.wait_send()
+    if relayed:
+        for over, straight, at_end, parity in returned:
+            pl.when(at_end & (side == parity))(over.wait_send)
+    parts_of_bases.drain()
+    weights.drain()
 
 
 def exchange(fs, tp, mixer, cell, grads, bases, weights, means, olds):
@@ -552,8 +607,8 @@
             pltpu.VMEM((tp - 1, 8, 128), f32),
             dma((3, CHUNKS, max(15, fs - 1))),
             dma((3, CHUNKS, max(13, fs - 1))),
-            dma((2, fs - 1)),
-            dma((2, fs - 1)),
+            dma((2, 1, max(15, fs - 1))),
+            dma((2, 1, max(13, fs - 1))),
             dma((2, max(1, tp // 2 - 1))),
             dma((2, max(1, tp // 2 - 1))),
             dma((2,)),
@@ -561,7 +616,8 @@
             dma((fs - 1,)),
             dma((fs - 1,)),
             dma((fs - 1,)),
-            dma((fs - 1,)),
+            dma((owners,)),
+            dma((owners,)),
             dma((tp - 1,)),
             dma((tp - 1,)),
             dma((17,)),

time: 156 us -> 151 us (0.968)
  Pallas kernels: 155 us -> 150 us
    pallas_call x1, Pallas kernels: 148 us -> 144 us  [exchange(): pl.pallas_call(functools.partial(kernel, fs, tp, owners), out_shape=(*(wh...]
where the time goes in v3:
time: 151 us
  Pallas kernels  150 us (99%)
    pallas_call x1, Pallas kernels, exchange(): pl.pallas_call(functools.partial(kernel, fs, tp, owners), out_shape=(*(wh...  144 us
    pallas_call x1, Pallas kernels, local(): pl.pallas_call(functools.partial(last_kernel, entries), out_shape=shapes,...  6.72 us

profile of v3, /device:TPU:0, one launch (start us, length us, event | category | flops | bytes accessed | tf_op | source)
XLA Modules:
  0.0 151.1 jit_solution(10531287116094371310)
XLA Ops:
  0.7 143.7 %shard_map.256 = (bf16[4096,512]{1,0:T(8,128)(2,1)S(1)}, bf16[4096,512]{1,0:T(8,128)(2,1)S(1)}, bf16[2048,1024]{1,0:T(8,128)(2,1)S(1)}, bf16[8,2,2,128,256]{4,3,...) custom-call(bf16[1024,4096]{1,0:T(8,128)(2,1)} %mixer_hbm.1, ...), custom_call_target="tpu_custom_call" | custom-call | tf_op jit(solution)/shard_map/pallas_call | solution.py:585
  144.3 6.7 %shard_map.257 = (f32[512,512]{1,0:T(8,128)}, f32[512,512]{1,0:T(8,128)}, f32[256,1024]{1,0:T(8,128)}, bf16[4096,512]{1,0:T(8,128)(2,1)}, bf16[4096,512]{1,0:T(8...) custom-call(bf16[4096,512]{1,0:T(8,128)(2,1)S(1)} %get-tuple-element, ...), custom_call_target="tpu_custom_call" | custom-call | tf_op jit(solution)/shard_map/pallas_call | solution.py:720

commit v4 on v3

--- a/solution.py
+++ b/solution.py
@@ -13,9 +13,8 @@
 learn_rate = 0.05
 
 MESH = pl.DeviceIdType.MESH
-LINE_CHUNKS = 7
-BASE_LINE = (False, True)
-CHUNKS = 4
+LINE_SHARE = 8 / 16
+BASE_LINES = (0, 1)
 
 
 def matmul(left, right):
@@ -33,10 +32,10 @@
 
 
 class Gather:
-    def __init__(self, fs, me, count, chunks, slot, line, send_sem, recv_sem):
-        self.fs, self.me, self.count, self.chunks = fs, me, count, chunks
-        self.slot, self.line = slot, line
-        self.send_sem, self.recv_sem = send_sem, recv_sem
+    def __init__(self, fs, me, refs, chunks, lines, piece, several, sems):
+        self.fs, self.me, self.refs, self.chunks = fs, me, refs, chunks
+        self.lines, self.piece, self.several = lines, piece, several
+        self.send_sem, self.step_sem, self.last_sem = sems
         self.relayed = fs == 8
         self.place, self.side = me // 2, lax.rem(me, 2)
 
@@ -44,45 +43,55 @@
         place = lax.rem(self.place + step + 4, 4)
         return place * 2 + (1 - self.side if other else self.side)
 
+    def arrival(self, w, i, role):
+        if self.relayed and role < 6:
+            return self.step_sem.at[w, (0, 2, 3, 1, 2, 3)[role], i]
+        return self.last_sem.at[w, role - 6 if self.relayed else role]
+
     def copy(self, w, i, origin, site, role, target):
-        return pltpu.make_async_remote_copy(
-            src_ref=self.slot(w, i, origin),
-            dst_ref=self.slot(w, i, origin),
-            send_sem=self.send_sem.at[w, i, site],
-            recv_sem=self.recv_sem.at[w, i, role],
-            device_id={"fs": target},
-            device_id_type=MESH,
-        )
-
-    def arrive(self, w, i, origin, role, inside=True):
+        return remote(
+            self.piece(w, origin, i),
+            self.piece(w, origin, i),
+            self.send_sem.at[w, site],
+            self.arrival(w, i, role),
+            fs=target,
+        )
+
+    def total(self, w, origin, count, site, role):
+        return remote(
+            self.several(w, origin, count),
+            self.several(w, origin, count),
+            self.send_sem.at[w, site],
+            self.arrival(w, 0, role),
+            fs=lax.rem(self.me + 1, self.fs),
+        )
+
+    def arrive(self, w, i, origin, role, inside):
         copy = self.copy(w, i, origin, 0, role, lax.rem(self.me + 1, self.fs))
-        if inside is True:
-            copy.wait_recv()
-        else:
-            pl.when(inside)(copy.wait_recv)
+        pl.when(inside)(copy.wait_recv)
 
     def sites(self, w, i):
         p = self.place
-        line = self.line(w, i)
-        out = [
-            (0, self.me, 0, self.index(1), p < 3),
-            (1, self.me, 3, self.index(-1), p > 0),
-            (2, self.me, 6, self.index(0, True), True),
-        ]
+        line = i < self.lines[w]
         cross = self.index(0, True)
+        out = {
+            0: (self.me, 0, self.index(1), p < 3),
+            1: (self.me, 3, self.index(-1), p > 0),
+            2: (self.me, 6, cross, None),
+            13: (cross, 7, self.index(1), (p < 3) & (line | (p == 0))),
+            14: (cross, 10, self.index(-1), (p > 0) & (line | (p == 3))),
+        }
         for d in (1, 2):
-            out.append((2 + d, self.index(-d), d, self.index(1), (p >= d) & (p < 3)))
-            out.append((4 + d, self.index(d), 3 + d, self.index(-1), (p + d < 4) & (p > 0)))
+            out[2 + d] = (self.index(-d), d, self.index(1), (p >= d) & (p < 3))
+            out[4 + d] = (self.index(d), 3 + d, self.index(-1), (p + d < 4) & (p > 0))
         for d in (1, 2, 3):
             below, above = p >= d, p + d < 4
             if d == 1:
                 below = below & jnp.logical_not(line | (p == 1))
                 above = above & jnp.logical_not(line | (p == 2))
-            out.append((6 + d, self.index(-d), 6 + d, cross, below))
-            out.append((9 + d, self.index(d), 9 + d, cross, above))
-        out.append((13, cross, 7, self.index(1), (p < 3) & (line | (p == 0))))
-        out.append((14, cross, 10, self.index(-1), (p > 0) & (line | (p == 3))))
-        return {site[0]: site for site in out}
+            out[6 + d] = (self.index(-d), 6 + d, cross, below)
+            out[9 + d] = (self.index(d), 9 + d, cross, above)
+        return out
 
     def direct(self):
         return [(k - 1, lax.rem(self.me + k, self.fs)) for k in range(1, self.fs)]
@@ -90,20 +99,20 @@
     def send(self, w, i, wanted, also=None):
         table = self.sites(w, i)
         for site in wanted:
-            number, origin, role, target, inside = table[site]
-            copy = self.copy(w, i, origin, number, role, target)
+            origin, role, target, inside = table[site]
+            copy = self.copy(w, i, origin, site, role, target)
             if also is not None:
                 inside = inside & also
-            if inside is True:
+            if inside is None:
                 copy.start()
             else:
                 pl.when(inside)(copy.start)
 
-    def each(self, step, low=0, high=None, only=None):
+    def each(self, step, low=0, high=None):
         high = self.chunks if high is None else high
 
         def chunk(i, carry):
-            for w in range(self.count) if only is None else (only,):
+            for w in range(len(self.refs)):
                 step(w, i)
             return carry
 
@@ -112,7 +121,7 @@
         elif high > low:
             lax.fori_loop(low, high, chunk, 0)
 
-    def start(self, low=0, high=None, only=None):
+    def start(self, low=0, high=None):
         def step(w, i):
             if self.relayed:
                 self.send(w, i, (0, 1, 2))
@@ -120,7 +129,7 @@
                 for number, target in self.direct():
                     self.copy(w, i, self.me, number, number, target).start()
 
-        self.each(step, low, high, only)
+        self.each(step, low, high)
 
     def relay_out(self, low=0, high=None):
         p = self.place
@@ -159,41 +168,52 @@
             self.each(step, low, high)
 
     def relay_cross(self):
-        def step(w, i):
-            self.arrive(w, i, self.index(0, True), 6)
-            self.send(w, i, (13, 14))
-
-        if self.relayed:
-            self.each(step)
+        if not self.relayed:
+            return
+        for w in range(len(self.refs)):
+            self.total(w, self.index(0, True), self.chunks, 0, 6).wait_recv()
+        self.each(lambda w, i: self.send(w, i, (13, 14)))
 
     def finish(self):
         p = self.place
-
-        def step(w, i):
+        for w in range(len(self.refs)):
             if not self.relayed:
                 for k in range(1, self.fs):
-                    self.arrive(w, i, lax.rem(self.me + self.fs - k, self.fs), k - 1)
-                return
+                    source = lax.rem(self.me + self.fs - k, self.fs)
+                    self.total(w, source, self.chunks, 0, k - 1).wait_recv()
+                continue
             for d in (1, 2, 3):
-                self.arrive(w, i, self.index(-d, True), 6 + d, p >= d)
-                self.arrive(w, i, self.index(d, True), 9 + d, p + d < 4)
-
-        self.each(step)
+                below = self.total(w, self.index(-d, True), self.chunks, 0, 6 + d)
+                above = self.total(w, self.index(d, True), self.chunks, 0, 9 + d)
+                pl.when(p >= d)(below.wait_recv)
+                pl.when(p + d < 4)(above.wait_recv)
 
     def drain(self):
-        def step(w, i):
+        p = self.place
+        for w in range(len(self.refs)):
             if not self.relayed:
-                for number, target in self.direct():
-                    self.copy(w, i, self.me, number, number, target).wait_send()
-                return
-            for number, origin, role, target, inside in self.sites(w, i).values():
-                copy = self.copy(w, i, origin, number, role, target)
-                if inside is True:
-                    copy.wait_send()
-                else:
-                    pl.when(inside)(copy.wait_send)
-
-        self.each(step)
+                for number, _ in self.direct():
+                    self.total(w, self.me, self.chunks, number, 0).wait_send()
+                continue
+            on_line, rest = self.lines[w], self.chunks - self.lines[w]
+            for site, (origin, _, _, inside) in self.sites(w, 0).items():
+                waits = [(self.chunks, inside)]
+                if site == 7:
+                    waits = [(rest, p >= 2)]
+                elif site == 10:
+                    waits = [(rest, p <= 1)]
+                elif site == 13:
+                    waits = [(self.chunks, p == 0), (on_line, (p > 0) & (p < 3))]
+                elif site == 14:
+                    waits = [(self.chunks, p == 3), (on_line, (p > 0) & (p < 3))]
+                for count, when in waits:
+                    if count == 0:
+                        continue
+                    copy = self.total(w, origin, count, site, 0)
+                    if when is None:
+                        copy.wait_send()
+                    else:
+                        pl.when(when)(copy.wait_send)
 
 
 def remote(ref_from, ref_to, send, recv, **device):
@@ -228,9 +248,7 @@
     qs_hbm,
     vs_hbm,
     os_hbm,
-    qw_all,
-    vw_all,
-    ow_all,
+    w_all,
     pair_all,
     ob_all,
     firsts,
@@ -253,9 +271,11 @@
     square_own,
     square_in,
     w_send,
-    w_recv,
+    w_step,
+    w_last,
     b_send,
-    b_recv,
+    b_step,
+    b_last,
     y_send,
     y_recv,
     c_send,
@@ -318,45 +338,49 @@
     for load in loads[:3]:
         load.wait()
     bases = (pair_all, ob_all)
-    wholes = (qw_all, vw_all, ow_all)
     sent = []
-
-    def base_slot(w, i, origin):
-        return bases[w].at[origin, far, core]
-
-    def weight_slot(w, i, origin):
-        block = wholes[w].shape[0] // fs
-        rows = block // CHUNKS
-        return wholes[w].at[aligned(origin * block + i * rows, rows), :]
-
     parts_of_bases = Gather(
-        fs, me, 2, 1, base_slot, lambda w, i: BASE_LINE[w], b_send, b_recv
+        fs,
+        me,
+        bases,
+        1,
+        BASE_LINES,
+        lambda w, origin, i: bases[w].at[origin, far, core],
+        lambda w, origin, count: bases[w].at[origin, far, core],
+        (b_send, b_step, b_last),
     )
+    chunks = w_all.shape[1]
     weights = Gather(
         fs,
         me,
-        3,
-        CHUNKS,
-        weight_slot,
-        lambda w, i: i * len(wholes) + w < LINE_CHUNKS,
-        w_send,
-        w_recv,
+        (w_all,),
+        chunks,
+        (int(LINE_SHARE * chunks),),
+        lambda w, origin, i: w_all.at[origin, i],
+        lambda w, origin, count: w_all.at[origin, pl.ds(0, count)],
+        (w_send, w_step, w_last),
     )
     parts_of_bases.start()
     for load in loads[3:6]:
         load.wait()
-    for own, whole in zip((qw, vw, ow), wholes):
-        block = own.shape[0]
-        whole[aligned(me * block, block), :] = own[...].astype(jnp.bfloat16)
-    weights.start(0, 1, 0)
+    across, spread = w_all.shape[4], ow.shape[1] // w_all.shape[4]
+    for n, own in enumerate((qw, vw)):
+        w_all[me, :, n] = own[...].astype(jnp.bfloat16).reshape(chunks, -1, across)
+    low_rows = w_all.shape[3] // spread
+    for h in range(spread):
+        piece = ow[:, h * across : (h + 1) * across].astype(jnp.bfloat16)
+        w_all[me, :, 2, h * low_rows : (h + 1) * low_rows, :] = piece.reshape(
+            chunks, low_rows, across
+        )
+    weights.start(0, 1)
     part[...] = jnp.zeros_like(part)
     parts_of_bases.relay(1)
     parts_of_bases.relay_cross()
-    weights.start(0, 1, 1)
+    weights.start(1, 2)
     parts_of_bases.relay(2)
-    weights.start(0, 1, 2)
+    weights.start(2, 3)
     parts_of_bases.relay(3)
-    weights.start(1)
+    weights.start(3)
     parts_of_bases.finish()
     for k in range(1, fars):
         for n, whole in enumerate(bases):
@@ -370,7 +394,7 @@
             )
             copy.start()
             sent.append(copy)
-    weights.relay_out(0, 2)
+    weights.relay_out(0, chunks // 2)
     for k in range(1, fars):
         source = lax.rem(far + fars - k, fars)
         for n, whole in enumerate(bases):
@@ -441,8 +465,8 @@
         pl.when(owns(target))(copy.start)
         drains.append((copy, owns(target)))
 
-    weights.relay_out(2)
-    weights.relay_in(0, 1)
+    weights.relay_out(chunks // 2)
+    weights.relay_in(0, chunks // 4)
 
     def gram(ref):
         rows, size = ref.shape[3], ref.shape[4]
@@ -500,7 +524,7 @@
     for copy, inside in back:
         pl.when(inside)(copy.start)
 
-    weights.relay_in(1)
+    weights.relay_in(chunks // 4)
     weights.relay(2)
     weights.relay_cross()
 
@@ -576,8 +600,8 @@
     hbm, vmem = pl.BlockSpec(memory_space=pltpu.HBM), pl.BlockSpec(memory_space=pltpu.VMEM)
     dma = pltpu.SemaphoreType.DMA
 
-    def whole(array):
-        return jax.ShapeDtypeStruct((array.shape[0] * fs, array.shape[1]), bf16)
+    rows, across = weights[0].shape
+    chunks = min(16, rows * across // (16 * weights[2].shape[1]))
 
     def parted(array, columns):
         return jax.ShapeDtypeStruct((fs, tp // 2, 2, array.shape[0] // tp, columns), bf16)
@@ -585,7 +609,7 @@
     return pl.pallas_call(
         functools.partial(kernel, fs, tp, owners),
         out_shape=(
-            *(whole(weight) for weight in weights),
+            jax.ShapeDtypeStruct((fs, chunks, 3, rows // chunks, across), bf16),
             parted(bases[0], 2 * rank),
             parted(bases[2], rank),
             jax.ShapeDtypeStruct((rank, total), f32),
@@ -594,7 +618,7 @@
             jax.ShapeDtypeStruct((8, 128), f32),
         ),
         in_specs=[hbm] * 17,
-        out_specs=(vmem,) * 9,
+        out_specs=(vmem,) * 7,
         scratch_shapes=[
             *(pltpu.VMEM(array.shape, bf16) for array in (mixer, cell, *grads)),
             *(pltpu.VMEM(array.shape, f32) for array in weights),
@@ -605,10 +629,12 @@
             pltpu.VMEM((fs - 1, rank // owners, total), f32),
             pltpu.VMEM((8, 128), f32),
             pltpu.VMEM((tp - 1, 8, 128), f32),
-            dma((3, CHUNKS, max(15, fs - 1))),
-            dma((3, CHUNKS, max(13, fs - 1))),
-            dma((2, 1, max(15, fs - 1))),
-            dma((2, 1, max(13, fs - 1))),
+            dma((1, max(15, fs - 1))),
+            dma((1, 4, chunks)),
+            dma((1, max(7, fs - 1))),
+            dma((2, max(15, fs - 1))),
+            dma((2, 4, 1)),
+            dma((2, max(7, fs - 1))),
             dma((2, max(1, tp // 2 - 1))),
             dma((2, max(1, tp // 2 - 1))),
             dma((2,)),
@@ -633,9 +659,9 @@
 
 
 def last_kernel(entries, *refs):
-    wholes, (pair, ob, firsts, seconds, dirs, squares) = refs[:3], refs[3:9]
-    outputs, stage, sem = refs[9:21], refs[21:27], refs[27]
-    rank = pair.shape[2] // 2
+    w_all, pair, ob, firsts, seconds, dirs, squares = refs[:7]
+    outputs, stage, sem = refs[7:19], refs[19:25], refs[25]
+    rank, across = pair.shape[2] // 2, w_all.shape[4]
     me = lax.axis_index("fs")
     copies = []
 
@@ -645,29 +671,31 @@
         copies.append(copy)
 
     cuts, left = [], 0
-    for whole in wholes:
-        cuts.append(pl.ds(left, whole.shape[1]))
-        left += whole.shape[1]
+    for output in outputs[:3]:
+        cuts.append((left, output.shape[1]))
+        left += output.shape[1]
     for n, cut in enumerate(cuts):
-        put(firsts.at[:, cut], outputs[6 + n])
-        put(seconds.at[:, cut], outputs[9 + n])
+        put(firsts.at[:, pl.ds(*cut)], outputs[6 + n])
+        put(seconds.at[:, pl.ds(*cut)], outputs[9 + n])
     factor = 1.0 / jnp.sqrt(squares[0:1, 0:1] / entries + floor_mean)
     scale = -learn_rate * factor
     bases = ((pair, 0), (pair, rank), (ob, 0))
     for n, (cut, (base, low)) in enumerate(zip(cuts, bases)):
-        both = dirs[:, cut]
+        both = dirs[:, pl.ds(*cut)]
         own = base[me, :, low : low + rank]
         stage[n][...] = -factor * matmul(jnp.concatenate([own, own], axis=1), both)
         put(stage[n], outputs[n])
-        high = both[:rank]
         block = base.shape[1]
+        rows = block // w_all.shape[1]
         for o in range(base.shape[0]):
-            rows = pl.ds(o * block, block)
-            update = matmul(base[o, :, low : low + rank], high)
-            stage[3 + n][rows, :] = (
-                wholes[n][rows, :].astype(jnp.float32) + scale * update
-            ).astype(jnp.bfloat16)
-            put(stage[3 + n].at[rows, :], outputs[3 + n].at[rows, :])
+            update = scale * matmul(base[o, :, low : low + rank], both[:rank])
+            for h in range(cut[1] // across):
+                held = w_all[o, :, n, h * rows : (h + 1) * rows, :].reshape(block, across)
+                stage[3 + n][pl.ds(o * block, block), h * across : (h + 1) * across] = (
+                    held.astype(jnp.float32) + update[:, h * across : (h + 1) * across]
+                ).astype(jnp.bfloat16)
+            at = pl.ds(o * block, block)
+            put(stage[3 + n].at[at, :], outputs[3 + n].at[at, :])
     for copy in copies:
         copy.wait()
 
@@ -695,7 +723,7 @@
         means = (query_mean, value_mean, output_mean)
         olds = (query_square, value_square, output_square)
         weights = (query_weight, value_weight, output_weight)
-        *wholes, pair, ob, firsts, seconds, dirs, squares = exchange(
+        w_all, pair, ob, *rest = exchange(
             fs,
             tp,
             mixer_input,
@@ -712,7 +740,7 @@
         f32 = jnp.float32
         shapes = (
             *(jax.ShapeDtypeStruct(w.shape, f32) for w in weights),
-            *(jax.ShapeDtypeStruct(w.shape, w.dtype) for w in wholes),
+            *(jax.ShapeDtypeStruct((w.shape[0] * fs, w.shape[1]), jnp.bfloat16) for w in weights),
             *(jax.ShapeDtypeStruct(m.shape, f32) for m in means),
             *(jax.ShapeDtypeStruct(m.shape, f32) for m in olds),
         )
@@ -720,14 +748,14 @@
         return pl.pallas_call(
             functools.partial(last_kernel, entries),
             out_shape=shapes,
-            in_specs=[vmem] * 9,
+            in_specs=[vmem] * 7,
             out_specs=(pl.BlockSpec(memory_space=pl.ANY),) * 12,
             scratch_shapes=[
                 *(pltpu.VMEM(s.shape, s.dtype) for s in shapes[:6]),
                 pltpu.SemaphoreType.DMA((9 + 3 * fs,)),
             ],
             compiler_params=pltpu.CompilerParams(vmem_limit_bytes=VMEM_LAST),
-        )(*wholes, pair, ob, firsts, seconds, dirs, squares)
+        )(w_all, pair, ob, *rest)
 
     return local
 

time: 151 us -> 147 us (0.974); the launches traced: 151 us -> 145 us
  Pallas kernels: 150 us -> 145 us
    pallas_call x1, Pallas kernels: 144 us -> 138 us  [exchange(): pl.pallas_call(functools.partial(kernel, fs, tp, owners), out_shape=(jax....]
where the time goes in v4:
time: 147 us; the launch traced here: 145 us
  Pallas kernels  145 us (99%)
    pallas_call x1, Pallas kernels, exchange(): pl.pallas_call(functools.partial(kernel, fs, tp, owners), out_shape=(jax....  138 us
    pallas_call x1, Pallas kernels, local(): pl.pallas_call(functools.partial(last_kernel, entries), out_shape=shapes,...  6.42 us

profile of v4, /device:TPU:0, one launch (start us, length us, event | category | flops | bytes accessed | tf_op | source)
XLA Modules:
  0.0 145.3 jit_solution(111684738493276461)
XLA Ops:
  0.7 138.2 %shard_map.256 = (bf16[8,16,3,32,512]{4,3,2,1,0:T(8,128)(2,1)S(1)}, bf16[8,2,2,128,256]{4,3,2,1,0:T(8,128)(2,1)S(1)}, bf16[8,2,2,64,128]{4,3,2,1,0:T(8,128)(2,1)...) custom-call(bf16[1024,4096]{1,0:T(8,128)(2,1)} %mixer_hbm.1, ...), custom_call_target="tpu_custom_call" | custom-call | tf_op jit(solution)/shard_map/pallas_call | solution.py:609
  138.8 6.4 %shard_map.257 = (f32[512,512]{1,0:T(8,128)}, f32[512,512]{1,0:T(8,128)}, f32[256,1024]{1,0:T(8,128)}, bf16[4096,512]{1,0:T(8,128)(2,1)}, bf16[4096,512]{1,0:T(8...) custom-call(bf16[8,16,3,32,512]{4,3,2,1,0:T(8,128)(2,1)S(1)} %get-tu, ...), custom_call_target="tpu_custom_call" | custom-call | tf_op jit(solution)/shard_map/pallas_call | solution.py:748

commit v5 on v4

--- a/solution.py
+++ b/solution.py
@@ -325,15 +325,28 @@
         load.start()
 
     barrier = pltpu.get_barrier_semaphore()
-    for k in range(1, fs):
+
+    def greet(target):
         pl.semaphore_signal(
-            barrier, inc=1, device_id={"fs": lax.rem(me + k, fs)}, device_id_type=MESH
-        )
+            barrier, inc=1, device_id={"fs": target}, device_id_type=MESH
+        )
+
+    place = me // 2
     for k in range(1, tp):
         pl.semaphore_signal(
             barrier, inc=1, device_id={"tp": lax.rem(column + k, tp)}, device_id_type=MESH
         )
-    pl.semaphore_wait(barrier, fs + tp - 2)
+    if fs == 8:
+        greet(me + 1 - 2 * lax.rem(me, 2))
+        pl.when(place < 3)(lambda: greet(lax.rem(me + 2, fs)))
+        pl.when(place > 0)(lambda: greet(lax.rem(me + fs - 2, fs)))
+        inner = (place > 0) & (place < 3)
+        pl.when(inner)(lambda: pl.semaphore_wait(barrier, tp + 2))
+        pl.when(jnp.logical_not(inner))(lambda: pl.semaphore_wait(barrier, tp + 1))
+    else:
+        for k in range(1, fs):
+            greet(lax.rem(me + k, fs))
+        pl.semaphore_wait(barrier, fs + tp - 2)
 
     for load in loads[:3]:
         load.wait()

time: 147 us -> 145 us (0.986)
  Pallas kernels: 145 us -> 143 us
where the time goes in v5:
time: 145 us; the launch traced here: 144 us
  Pallas kernels  143 us (99%)
    pallas_call x1, Pallas kernels, exchange(): pl.pallas_call(functools.partial(kernel, fs, tp, owners), out_shape=(jax....  137 us
    pallas_call x1, Pallas kernels, local(): pl.pallas_call(functools.partial(last_kernel, entries), out_shape=shapes,...  6.42 us

profile of v5, /device:TPU:0, one launch (start us, length us, event | category | flops | bytes accessed | tf_op | source)
XLA Modules:
  0.0 143.8 jit_solution(17997511160642821516)
XLA Ops:
  0.7 136.8 %shard_map.256 = (bf16[8,16,3,32,512]{4,3,2,1,0:T(8,128)(2,1)S(1)}, bf16[8,2,2,128,256]{4,3,2,1,0:T(8,128)(2,1)S(1)}, bf16[8,2,2,64,128]{4,3,2,1,0:T(8,128)(2,1)...) custom-call(bf16[1024,4096]{1,0:T(8,128)(2,1)} %mixer_hbm.1, ...), custom_call_target="tpu_custom_call" | custom-call | tf_op jit(solution)/shard_map/pallas_call | solution.py:622
  137.4 6.4 %shard_map.257 = (f32[512,512]{1,0:T(8,128)}, f32[512,512]{1,0:T(8,128)}, f32[256,1024]{1,0:T(8,128)}, bf16[4096,512]{1,0:T(8,128)(2,1)}, bf16[4096,512]{1,0:T(8...) custom-call(bf16[8,16,3,32,512]{4,3,2,1,0:T(8,128)(2,1)S(1)} %get-tu, ...), custom_call_target="tpu_custom_call" | custom-call | tf_op jit(solution)/shard_map/pallas_call | solution.py:761

commit v6 on v5

--- a/solution.py
+++ b/solution.py
@@ -29,6 +29,10 @@
 
 def aligned(start, size):
     return pl.ds(pl.multiple_of(start, size), size)
+
+
+ARRIVE = (0, 1, 2, 2, 1, 0, 0, 1, 2, 3, 3, 2, 1)
+LEAVE = (0, 1, 2, 3, 4, 5, 4, 6, 7, 8, 8, 7, 6, 9, 10)
 
 
 class Gather:
@@ -45,14 +49,17 @@
 
     def arrival(self, w, i, role):
         if self.relayed and role < 6:
-            return self.step_sem.at[w, (0, 2, 3, 1, 2, 3)[role], i]
-        return self.last_sem.at[w, role - 6 if self.relayed else role]
+            return self.step_sem.at[w, ARRIVE[role], i]
+        return self.last_sem.at[w, ARRIVE[role] if self.relayed else role]
+
+    def departure(self, w, site):
+        return self.send_sem.at[w, LEAVE[site] if self.relayed else site]
 
     def copy(self, w, i, origin, site, role, target):
         return remote(
             self.piece(w, origin, i),
             self.piece(w, origin, i),
-            self.send_sem.at[w, site],
+            self.departure(w, site),
             self.arrival(w, i, role),
             fs=target,
         )
@@ -61,7 +68,7 @@
         return remote(
             self.several(w, origin, count),
             self.several(w, origin, count),
-            self.send_sem.at[w, site],
+            self.departure(w, site),
             self.arrival(w, 0, role),
             fs=lax.rem(self.me + 1, self.fs),
         )
@@ -642,12 +649,12 @@
             pltpu.VMEM((fs - 1, rank // owners, total), f32),
             pltpu.VMEM((8, 128), f32),
             pltpu.VMEM((tp - 1, 8, 128), f32),
-            dma((1, max(15, fs - 1))),
-            dma((1, 4, chunks)),
-            dma((1, max(7, fs - 1))),
-            dma((2, max(15, fs - 1))),
-            dma((2, 4, 1)),
-            dma((2, max(7, fs - 1))),
+            dma((1, max(11, fs - 1))),
+            dma((1, 3, chunks)),
+            dma((1, max(4, fs - 1))),
+            dma((2, max(11, fs - 1))),
+            dma((2, 3, 1)),
+            dma((2, max(4, fs - 1))),
             dma((2, max(1, tp // 2 - 1))),
             dma((2, max(1, tp // 2 - 1))),
             dma((2,)),

time: 145 us -> 145 us (level)
  no operation moved by 1% of the time
where the time goes in v6:
time: 145 us; the launch traced here: 144 us
  Pallas kernels  143 us (99%)
    pallas_call x1, Pallas kernels, exchange(): pl.pallas_call(functools.partial(kernel, fs, tp, owners), out_shape=(jax....  136 us
    pallas_call x1, Pallas kernels, local(): pl.pallas_call(functools.partial(last_kernel, entries), out_shape=shapes,...  6.42 us

profile of v6, /device:TPU:0, one launch (start us, length us, event | category | flops | bytes accessed | tf_op | source)
XLA Modules:
  0.0 143.6 jit_solution(7665592377113472186)
XLA Ops:
  0.7 136.5 %shard_map.256 = (bf16[8,16,3,32,512]{4,3,2,1,0:T(8,128)(2,1)S(1)}, bf16[8,2,2,128,256]{4,3,2,1,0:T(8,128)(2,1)S(1)}, bf16[8,2,2,64,128]{4,3,2,1,0:T(8,128)(2,1)...) custom-call(bf16[1024,4096]{1,0:T(8,128)(2,1)} %mixer_hbm.1, ...), custom_call_target="tpu_custom_call" | custom-call | tf_op jit(solution)/shard_map/pallas_call | solution.py:629
  137.1 6.4 %shard_map.257 = (f32[512,512]{1,0:T(8,128)}, f32[512,512]{1,0:T(8,128)}, f32[256,1024]{1,0:T(8,128)}, bf16[4096,512]{1,0:T(8,128)(2,1)}, bf16[4096,512]{1,0:T(8...) custom-call(bf16[8,16,3,32,512]{4,3,2,1,0:T(8,128)(2,1)S(1)} %get-tu, ...), custom_call_target="tpu_custom_call" | custom-call | tf_op jit(solution)/shard_map/pallas_call | solution.py:768
